TPU v7x, 32 devices: a whole 2x2x4 slice. The times are simulated.
32 devices in a mesh: sp: 8 (over z, x), tp: 4 (over y, core).
Axes of the slice: x: 2, y: 2, z: 4, core: 2. Of those that a mesh axis runs over, the one named last changes fastest.
Arguments:
- layer_grad: bfloat16 [2048, 2048], P('sp', 'tp'), may hold values from -6 to 6
- routes: int32 [2048, 2], P('sp'), may hold values from 0 to 7, all different within a row; in each aligned block of 256 rows (0 to 255, 256 to 511, ...) at most 96 rows name the same one
- route_weights: float32 [2048, 2], P('sp'), may hold values from 0.1 to 0.9
- expert_in: bfloat16 [8, 768, 2048], P('sp', None, 'tp'), may hold values from -50 to 50
- w_gate: bfloat16 [8, 2048, 2048], P('sp', None, 'tp'), may hold values from -0.125 to 0.125
- w_up: bfloat16 [8, 2048, 2048], P('sp', None, 'tp'), may hold values from -0.125 to 0.125
- w_down: bfloat16 [8, 2048, 2048], P('sp', 'tp'), may hold values from -0.125 to 0.125
- conv_in: bfloat16 [2048, 512], P('sp', 'tp'), may hold values from -6 to 6
- c_gate: bfloat16 [2048, 512], P('sp', 'tp'), may hold values from -6 to 6
- b_gate: bfloat16 [2048, 512], P('sp', 'tp'), may hold values from -1.5 to 1.5
- conv_out: bfloat16 [2048, 512], P('sp', 'tp'), may hold values from -1.5 to 1.5
- taps: bfloat16 [3, 512], P(None, 'tp'), may hold values from -3.5 to 3.5
- w_out: bfloat16 [512, 2048], P('tp'), may hold values from -0.25 to 0.25
Outputs:
- grad_w_gate: bfloat16 [8, 2048, 2048], P('sp', None, 'tp')
- grad_w_up: bfloat16 [8, 2048, 2048], P('sp', None, 'tp')
- grad_w_down: bfloat16 [8, 2048, 2048], P('sp', 'tp')
- grad_routed: bfloat16 [2048, 2048], P('sp', 'tp')
- grad_out_proj: float32 [512, 2048], P('tp', 'sp')
- grad_conv_in: bfloat16 [2048, 512], P('sp', 'tp')
- grad_c_gate: bfloat16 [2048, 512], P('sp', 'tp')
- grad_b_gate: bfloat16 [2048, 512], P('sp', 'tp')
Inputs may be any that keep to these rules, and one draw needn't show every extreme that they name: `routes`: each token names 2 different experts. Among the tokens of one block of 256, no expert is named more than 96 times, a bound that some block reaches.
All inputs are finite; a program needn't handle non-finite values.
Results may differ from a plain program's by a relative error of at most 0.019.
Values may be sent and summed in bfloat16 or wider, within the bound.
No kernel may reach another device: no remote copies, remote signals or barrier semaphores. Data moves between devices by JAX's collectives and lax.ppermute only.
A program may use at most 64 MiB of HBM per device.

v0:
```python
import jax
import jax.numpy as jnp
from jax import lax
from jax.sharding import PartitionSpec as P

clamp_limit = 7.0
swish_alpha = 1.702


def passed_along(value, axis, steps):
    count = lax.axis_size(axis)
    leading, last = (max(0, -steps), min(count, count - steps))
    return lax.ppermute(value, axis, [(source, source + steps) for source in range(leading, last)])


def per_device(
    layer_grad,
    routes,
    route_weights,
    expert_in,
    w_gate,
    w_up,
    w_down,
    conv_in,
    c_gate,
    b_gate,
    conv_out,
    taps,
    w_out,
):
    sp_devices = lax.axis_size("sp")
    tok_rows = layer_grad.shape[0]
    top_count = routes.shape[1]
    capacity = expert_in.shape[1] // sp_devices
    full_grad = lax.all_gather(layer_grad, "tp", axis=1, tiled=True)
    flat_routes = routes.reshape(-1)
    onehot = (flat_routes[:, None] == jnp.arange(sp_devices, dtype=jnp.int32)[None, :]).astype(
        jnp.int32
    )
    slot_rank = jnp.sum((jnp.cumsum(onehot, axis=0) - 1) * onehot, axis=1)
    slot_index = flat_routes * capacity + slot_rank
    weights = route_weights[:, :, None]
    scaled = (weights * layer_grad[:, None, :].astype(jnp.float32)).astype(jnp.bfloat16)
    scaled = scaled.reshape(tok_rows * top_count, -1)
    buffer = (
        jnp.zeros((sp_devices * capacity, scaled.shape[1]), jnp.bfloat16).at[slot_index].set(scaled)
    )
    arrived = lax.all_to_all(
        buffer.reshape(sp_devices, capacity, -1), "sp", split_axis=0, concat_axis=0, tiled=True
    )
    expert_grad, saved_rows = (
        lax.all_gather(arrived.reshape(sp_devices * capacity, -1), "tp", axis=1, tiled=True),
        lax.all_gather(expert_in[0], "tp", axis=1, tiled=True),
    )
    gate_weight = w_gate[0]
    up_weight = w_up[0]
    down_weight = w_down[0]
    gate_pre = jnp.dot(saved_rows, gate_weight, preferred_element_type=jnp.float32)
    up_pre = jnp.dot(saved_rows, up_weight, preferred_element_type=jnp.float32)
    gate_cut = jnp.minimum(gate_pre, clamp_limit)
    up_cut = jnp.clip(up_pre, -clamp_limit, clamp_limit)
    sigmoid_gate = jax.nn.sigmoid(swish_alpha * gate_cut)
    hidden = ((up_cut + 1.0) * gate_cut * sigmoid_gate).astype(jnp.bfloat16)
    act_grad = jnp.einsum("rd,fd->rf", expert_grad, down_weight, preferred_element_type=jnp.float32)
    grad_down = jnp.einsum(
        "rf,rd->fd", hidden, expert_grad, preferred_element_type=jnp.float32
    ).astype(jnp.bfloat16)
    slope = sigmoid_gate + swish_alpha * gate_cut * sigmoid_gate * (1.0 - sigmoid_gate)
    gate_grad = jnp.where(gate_pre < clamp_limit, act_grad * (up_cut + 1.0) * slope, 0.0).astype(
        jnp.bfloat16
    )
    up_grad = jnp.where(
        jnp.abs(up_pre) < clamp_limit, act_grad * gate_cut * sigmoid_gate, 0.0
    ).astype(jnp.bfloat16)
    grad_gate = jnp.einsum(
        "rd,rf->df", saved_rows, gate_grad, preferred_element_type=jnp.float32
    ).astype(jnp.bfloat16)
    grad_up = jnp.einsum(
        "rd,rf->df", saved_rows, up_grad, preferred_element_type=jnp.float32
    ).astype(jnp.bfloat16)
    partial_value = jnp.einsum(
        "rf,df->rd", gate_grad, gate_weight, preferred_element_type=jnp.float32
    )
    partial_value = partial_value + jnp.einsum(
        "rf,df->rd", up_grad, up_weight, preferred_element_type=jnp.float32
    )
    rounded_terms = partial_value.astype(jnp.bfloat16)
    reduced = (
        lax.psum_scatter(rounded_terms, "tp", scatter_dimension=1, tiled=True)
        .astype(jnp.float32)
        .astype(jnp.bfloat16)
    )
    returned = lax.all_to_all(
        reduced.reshape(sp_devices, capacity, -1), "sp", split_axis=0, concat_axis=0, tiled=True
    )
    returned = returned.reshape(sp_devices * capacity, -1)
    picked = returned[slot_index]
    picked = picked.reshape(tok_rows, top_count, -1)
    grad_routed = jnp.sum(picked.astype(jnp.float32), axis=1).astype(jnp.bfloat16)
    mixer_grad = jnp.einsum("td,cd->tc", full_grad, w_out, preferred_element_type=jnp.float32)
    mixed = (b_gate.astype(jnp.float32) * conv_out.astype(jnp.float32)).astype(jnp.bfloat16)
    projected = lax.psum_scatter(
        jnp.einsum("td,tc->dc", full_grad, mixed, preferred_element_type=jnp.float32),
        "sp",
        scatter_dimension=0,
        tiled=True,
    )
    grad_out_proj = projected.T
    out_grad = mixer_grad * b_gate.astype(jnp.float32)
    tap_reach = taps.shape[0] - 1
    following = passed_along(out_grad[:tap_reach], "sp", -1)
    extended = jnp.concatenate([out_grad, following], axis=0)
    tap_values = taps.astype(jnp.float32)
    conv_grad = jnp.zeros_like(out_grad)
    for tap_index in range(tap_reach + 1):
        offset = tap_reach - tap_index
        conv_grad = conv_grad + tap_values[tap_index] * extended[offset : offset + tok_rows]
    grad_conv_in = (conv_grad * c_gate.astype(jnp.float32)).astype(jnp.bfloat16)
    grad_c_gate = (conv_grad * conv_in.astype(jnp.float32)).astype(jnp.bfloat16)
    grad_b_gate = (mixer_grad * conv_out.astype(jnp.float32)).astype(jnp.bfloat16)
    return (
        grad_gate[None],
        grad_up[None],
        grad_down[None],
        grad_routed,
        grad_out_proj,
        grad_conv_in,
        grad_c_gate,
        grad_b_gate,
    )


def solution(mesh):
    in_specs = (
        P("sp", "tp"),
        P("sp", None),
        P("sp", None),
        P("sp", None, "tp"),
        P("sp", None, "tp"),
        P("sp", None, "tp"),
        P("sp", "tp", None),
        P("sp", "tp"),
        P("sp", "tp"),
        P("sp", "tp"),
        P("sp", "tp"),
        P(None, "tp"),
        P("tp", None),
    )
    out_specs = (
        P("sp", None, "tp"),
        P("sp", None, "tp"),
        P("sp", "tp", None),
        P("sp", "tp"),
        P("tp", "sp"),
        P("sp", "tp"),
        P("sp", "tp"),
        P("sp", "tp"),
    )
    return jax.shard_map(
        per_device, mesh=mesh, in_specs=in_specs, out_specs=out_specs, check_vma=False
    )
```

profile of v0, /device:TPU:0, one launch (start us, length us, event | category | flops | bytes accessed | tf_op | source)
XLA Modules:
  0.0 212.0 jit_solution(14027986862488300360)
XLA Ops:
  11.5 2.2 %mul.116 = f32[256,2,512]{2,1,0:T(2,128)} broadcast(bf16[256,512]{1,0:T(8,128)(2,1)} %param.13), dimensions={0,2} | broadcast | bytes 1310720 | tf_op jit(solution)/shard_map/mul | solution.py:43
  13.7 1.9 mul.117
  16.0 3.4 %scatter_custom_fusion = bf16[768,512]{1,0:T(8,128)(2,1)} fusion(s32[512]{0:T(512)S(1)} %bitcast.76, f32[512,512]{1,0:T(8,128)S(1)} %mul.117, f32[512]{0:T(512)S(1)} %mul.114, bf16[]{:T(256)} %constant.11.clone.1), kind=kCustom, calls=%fused_computation.36 | custom fusion | flops 524288 | bytes 1837058 | tf_op jit(solution)/shard_map/scatter | solution.py:46
  19.4 27.5 %all_to_all.10 = bf16[8,96,512]{2,1,0:T(8,128)(2,1)} all-to-all(bf16[8,96,512]{2,1,0:T(8,128)(2,1)} %bitcast.73), channel_id=1, replica_groups=mesh['sp'=8,'tp'=4] {'sp'}, dimensions={0} | all-to-all | bytes 1572864 | tf_op jit(solution)/shard_map/all_to_all | solution.py:48
  48.0 5.6 %fusion.4 = f32[768,512]{1,0:T(8,128)} fusion(bf16[1,768,2048]{2,1,0:T(8,128)(2,1)} %all-gather.9.cloned.1.call-done, bf16[1,2048,512]{2,1,0:T(8,128)(2,1)} %param.18), kind=kOutput, calls=%fused_computation.7 | convolution fusion | flops 1610612736 | bytes 6815744 | tf_op jit(solution)/shard_map/dot_general | solution.py:59
  53.6 3.0 %fusion.6 = f32[768,512]{1,0:T(8,128)} fusion(bf16[1,768,2048]{2,1,0:T(8,128)(2,1)S(1)} %copy-done.1, bf16[1,2048,512]{2,1,0:T(8,128)(2,1)S(1)} %copy-done), kind=kOutput, calls=%fused_computation.9 | convolution fusion | flops 1610612736 | bytes 6815744 | tf_op jit(solution)/shard_map/dot_general | solution.py:58
  56.6 18.1 %all-gather.5.cloned.1.call-done = bf16[768,2048]{1,0:T(8,128)(2,1)} async-done(((bf16[768,512]{1,0:T(8,128)(2,1)}), bf16[768,2048]{1,0:T(8,128)(2,1)}) %all-gather.5.cloned.1.call-update) | async-done | bytes 3145744 | tf_op jit(solution)/shard_map/all_gather | solution.py:52
  74.7 6.1 %select_convert_fusion = (bf16[768,512]{1,0:T(8,128)(2,1)S(1)}, bf16[768,512]{1,0:T(8,128)(2,1)S(1)}) fusion(f32[768,512]{1,0:T(8,128)} %fusion.4, f32[768,512]{1,0:T(8,128)} %fusion.6, bf16[768,2048]{1,0:T(8,128)(2,1)} %all-gather.5.cloned.1.call-done, bf16[1,512,2048]{2,1,0:T(8,128)(2,1)} %param.19), kind=kOutput, calls=%fused_computation.26 | convolution fusion | flops 1619263488 | bytes 9961472 | tf_op jit(solution)/shard_map/rd,fd->rf/dot_general | solution.py:64
  80.8 1.8 fusion.25
  83.0 3.5 %add_convert_fusion = bf16[768,2048]{1,0:T(8,128)(2,1)} fusion(f32[768,2048]{1,0:T(8,128)S(1)} %fusion.25, bf16[768,512]{1,0:T(8,128)(2,1)S(1)} %get-tuple-element.26, bf16[1,2048,512]{2,1,0:T(8,128)(2,1)S(1)} %copy-done.5), kind=kOutput, calls=%fused_computation.2 | convolution fusion | flops 1613758464 | bytes 12320768 | tf_op jit(solution)/shard_map/rf,df->rd/dot_general | solution.py:84
  87.3 5.7 %all-gather.7.cloned.1.call-done = bf16[256,2048]{1,0:T(8,128)(2,1)} async-done(((bf16[256,512]{1,0:T(8,128)(2,1)}), bf16[256,2048]{1,0:T(8,128)(2,1)}) %all-gather.7.cloned.1.call-update) | async-done | bytes 1048592 | tf_op jit(solution)/shard_map/all_gather | solution.py:35
  93.0 2.4 %fusion.40 = (bf16[256,128]{1,0:T(8,128)(2,1)}, f32[256,128]{1,0:T(8,128)S(1)}) fusion(bf16[256,128]{1,0:T(8,128)(2,1)S(1)} %copy-done.7, bf16[256,128]{1,0:T(8,128)(2,1)S(1)} %copy-done.8, bf16[256,2048]{1,0:T(8,128)(2,1)} %all-gather.7.cloned.1.call-done, bf16[128,2048]{1,0:T(8,128)(2,1)S(1)} %copy-done.6), kind=kOutput, calls=%fused_computation.49 | convolution fusion | flops 134381568 | bytes 1900544 | tf_op jit(solution)/shard_map/td,cd->tc/dot_general | solution.py:100
  95.4 1.4 collective-permute-start
  98.2 2.7 %collective-permute-done = f32[2,128]{1,0:T(2,128)S(1)} collective-permute-done((f32[2,128]{1,0:T(2,128)S(1)}, f32[2,128]{1,0:T(2,128)S(1)}, u32[]{:S(2)}, u32[]{:S(2)}) %collective-permute-start) | collective-permute-done | bytes 1056 | tf_op jit(solution)/shard_map/ppermute | solution.py:13
  102.3 30.8 %reduce-scatter.3.cloned.1.call-done = bf16[768,512]{1,0:T(8,128)(2,1)} async-done(((bf16[768,2048]{1,0:T(8,128)(2,1)}), bf16[768,512]{1,0:T(8,128)(2,1)}) %reduce-scatter.3.cloned.1.call-update) | async-done | bytes 786448 | tf_op jit(solution)/shard_map/reduce_scatter | solution.py:89
  133.1 5.5 %all-to-all-start.1 = ((bf16[8,96,512]{2,1,0:T(8,128)(2,1)}), bf16[8,96,512]{2,1,0:T(8,128)(2,1)S(1)}, u32[]{:S(2)}, u32[]{:S(2)}) async-start(bf16[8,96,512]{2,1,0:T(8,128)(2,1)} %bitcast.75), calls=%async_computation.2 | async-start | bytes 1572864 | tf_op jit(solution)/shard_map/all_to_all | solution.py:93
  138.6 5.3 %fusion.18 = bf16[1,2048,512]{1,2,0:T(8,128)(2,1)} fusion(bf16[768,512]{1,0:T(8,128)(2,1)} %copy-done.4, bf16[1,768,2048]{2,1,0:T(8,128)(2,1)} %all-gather.9.cloned.1.call-done), kind=kOutput, calls=%fused_computation.16 | convolution fusion | flops 1611661312 | bytes 6029312 | tf_op jit(solution)/shard_map/rd,rf->df/dot_general | solution.py:75
  143.9 3.9 %copy.27 = bf16[1,2048,512]{2,1,0:T(8,128)(2,1)} copy(bf16[1,2048,512]{1,2,0:T(8,128)(2,1)} %fusion.18) | data formatting | bytes 4194304
  147.8 5.3 %fusion.15 = bf16[1,2048,512]{1,2,0:T(8,128)(2,1)} fusion(bf16[768,512]{1,0:T(8,128)(2,1)} %copy-done.3, bf16[1,768,2048]{2,1,0:T(8,128)(2,1)} %all-gather.9.cloned.1.call-done), kind=kOutput, calls=%fused_computation.15 | convolution fusion | flops 1611661312 | bytes 6029312 | tf_op jit(solution)/shard_map/rd,rf->df/dot_general | solution.py:78
  153.1 3.9 %copy.28 = bf16[1,2048,512]{2,1,0:T(8,128)(2,1)} copy(bf16[1,2048,512]{1,2,0:T(8,128)(2,1)} %fusion.15) | data formatting | bytes 4194304
  157.0 6.2 %fusion.14 = bf16[1,512,2048]{2,1,0:T(8,128)(2,1)} fusion(bf16[768,2048]{1,0:T(8,128)(2,1)} %all-gather.5.cloned.1.call-done, f32[768,512]{1,0:T(8,128)} %fusion.6, f32[768,512]{1,0:T(8,128)} %fusion.4), kind=kOutput, calls=%fused_computation.14 | convolution fusion | flops 1615593472 | bytes 8388608 | tf_op jit(solution)/shard_map/rf,rd->fd/dot_general | solution.py:65
  164.6 2.0 gather_fusion
  166.7 2.1 reduce_sum.25
  168.8 36.7 %reduce-scatter.5.cloned.1.call-done = f32[256,128]{0,1:T(8,128)} async-done(((f32[2048,128]{0,1:T(8,128)}), f32[256,128]{0,1:T(8,128)}) %reduce-scatter.5.cloned.1.call-update) | async-done | bytes 131088 | tf_op jit(solution)/shard_map/reduce_scatter | solution.py:102
  (61 shorter events, 11.0 us)
Async XLA Ops:
  7.2 46.4 %copy-start = (bf16[1,2048,512]{2,1,0:T(8,128)(2,1)S(1)}, bf16[1,2048,512]{2,1,0:T(8,128)(2,1)}, u32[]{:S(2)}) copy-start(bf16[1,2048,512]{2,1,0:T(8,128)(2,1)} %param.17) | copy-start | bytes 6291460
  7.2 40.8 %all-gather.9.cloned.1.call-start = ((), (), s32[]{:S(2)}) async-start(), calls=%async_computation.8 | async-start | bytes 3932160 | tf_op jit(solution)/shard_map/all_gather | solution.py:53
  7.9 7.7 %copy-start.11 = (f32[256,2]{0,1:T(2,128)S(1)}, f32[256,2]{0,1:T(2,128)}, u32[]{:S(2)}) copy-start(f32[256,2]{0,1:T(2,128)} %param.15) | copy-start | bytes 6148
  7.9 66.7 %all-gather.5.cloned.1.call-start = ((), (), s32[]{:S(2)}) async-start(), calls=%async_computation.4 | async-start | bytes 3932160 | tf_op jit(solution)/shard_map/all_gather | solution.py:52
  47.0 46.0 %all-gather.7.cloned.1.call-start = ((), (), s32[]{:S(2)}) async-start(), calls=%async_computation.6 | async-start | bytes 1310720 | tf_op jit(solution)/shard_map/all_gather | solution.py:35
  47.7 85.4 %reduce-scatter.3.cloned.1.call-start = ((), (), s32[]{:S(2)}) async-start(), calls=%async_computation.5 | async-start | bytes 3932160 | tf_op jit(solution)/shard_map/reduce_scatter | solution.py:89
  47.9 5.6 %copy-start.1 = (bf16[1,768,2048]{2,1,0:T(8,128)(2,1)S(1)}, bf16[1,768,2048]{2,1,0:T(8,128)(2,1)}, u32[]{:S(2)}) copy-start(bf16[1,768,2048]{2,1,0:T(8,128)(2,1)} %all-gather.9.cloned.1.call-done) | copy-start | bytes 9437188
  80.8 1.9 copy-start.4
  80.8 1.9 copy-start.3
  80.8 2.2 %copy-start.5 = (bf16[1,2048,512]{2,1,0:T(8,128)(2,1)S(1)}, bf16[1,2048,512]{2,1,0:T(8,128)(2,1)}, u32[]{:S(2)}) copy-start(bf16[1,2048,512]{2,1,0:T(8,128)(2,1)} %param.18) | copy-start | bytes 6291460
  86.6 0.7 copy-start.12
  86.6 6.4 %copy-start.6 = (bf16[128,2048]{1,0:T(8,128)(2,1)S(1)}, bf16[128,2048]{1,0:T(8,128)(2,1)}, u32[]{:S(2)}) copy-start(bf16[128,2048]{1,0:T(8,128)(2,1)} %param.25) | copy-start | bytes 1572868
  86.6 6.4 %copy-start.7 = (bf16[256,128]{1,0:T(8,128)(2,1)S(1)}, bf16[256,128]{1,0:T(8,128)(2,1)}, u32[]{:S(2)}) copy-start(bf16[256,128]{1,0:T(8,128)(2,1)} %param.23) | copy-start | bytes 196612
  86.6 6.4 %copy-start.8 = (bf16[256,128]{1,0:T(8,128)(2,1)S(1)}, bf16[256,128]{1,0:T(8,128)(2,1)}, u32[]{:S(2)}) copy-start(bf16[256,128]{1,0:T(8,128)(2,1)} %param.22) | copy-start | bytes 196612
  86.6 118.9 %reduce-scatter.5.cloned.1.call-start = ((), (), s32[]{:S(2)}) async-start(), calls=%async_computation.7 | async-start | bytes 1179648 | tf_op jit(solution)/shard_map/reduce_scatter | solution.py:102
  93.0 3.8 %copy-start.2 = (bf16[256,2048]{1,0:T(8,128)(2,1)S(1)}, bf16[256,2048]{1,0:T(8,128)(2,1)}, u32[]{:S(2)}) copy-start(bf16[256,2048]{1,0:T(8,128)(2,1)} %all-gather.7.cloned.1.call-done) | copy-start | bytes 3145732
  95.4 5.6 %copy-start.9 = (bf16[256,128]{1,0:T(8,128)(2,1)S(1)}, bf16[256,128]{1,0:T(8,128)(2,1)}, u32[]{:S(2)}) copy-start(bf16[256,128]{1,0:T(8,128)(2,1)} %param.20) | copy-start | bytes 196612
  95.4 6.3 %copy-start.10 = (bf16[256,128]{1,0:T(8,128)(2,1)S(1)}, bf16[256,128]{1,0:T(8,128)(2,1)}, u32[]{:S(2)}) copy-start(bf16[256,128]{1,0:T(8,128)(2,1)} %param.21) | copy-start | bytes 196612
  95.4 5.6 %collective-permute-start = (f32[2,128]{1,0:T(2,128)S(1)}, f32[2,128]{1,0:T(2,128)S(1)}, u32[]{:S(2)}, u32[]{:S(2)}) collective-permute-start(f32[2,128]{1,0:T(2,128)S(1)} %slice.35), channel_id=1, source_target_pairs={{4,0},{8,4},{12,8},{16,12},{20,16},{24,20},{28,24},{5,1},{9,5},{13... | collective-permute-start | bytes 3080 | tf_op jit(solution)/shard_map/ppermute | solution.py:13
  133.1 31.5 %all-to-all-start.1 = ((bf16[8,96,512]{2,1,0:T(8,128)(2,1)}), bf16[8,96,512]{2,1,0:T(8,128)(2,1)S(1)}, u32[]{:S(2)}, u32[]{:S(2)}) async-start(bf16[8,96,512]{2,1,0:T(8,128)(2,1)} %bitcast.75), calls=%async_computation.2 | async-start | bytes 1572864 | tf_op jit(solution)/shard_map/all_to_all | solution.py:93
Sparse Core Ops, SparseCore 0:
  9.6 31.2 all-gather.8
  47.1 27.5 all-gather.4
  76.2 16.6 all-gather.6
  95.3 37.7 reduce-scatter.2
  136.9 68.5 reduce-scatter.4
where the time goes:
time: 213 us; the launch traced here: 212 us
  waiting for transfers between devices  96.8 us (45%)
  matrix products  40.6 us (19%)
  blocking collectives  27.5 us (13%)
  local copies, waits for them, and re-layouts  17 us (8%)
  between operations  14 us (7%)
  other arithmetic  8.79 us (4%)
  starting transfers between devices  7.3 us (3%)
    reduce_scatter x1, waiting for transfers between devices, per_device(): lax.psum_scatter(jnp.einsum('td,tc->dc', full_grad, mixed, preferred_elem...  36.7 us
    reduce_scatter x1, waiting for transfers between devices, per_device(): lax.psum_scatter(rounded_terms, 'tp', scatter_dimension=1, tiled=True)  30.8 us
    all_to_all x1, blocking collectives, per_device(): lax.all_to_all(buffer.reshape(sp_devices, capacity, -1), 'sp', split_axis...  27.5 us
    all_gather x1, waiting for transfers between devices, per_device(): lax.all_gather(arrived.reshape(sp_devices * capacity, -1), 'tp', axis=1,...  18.1 us
    unnamed x30, local copies, waits for them, and re-layouts  9.79 us
    dot_general x1, matrix products, per_device(): jnp.einsum('rf,rd->fd', hidden, expert_grad, preferred_element_type=jnp.f...  6.18 us
    dot_general x1, matrix products, per_device(): jnp.einsum('rd,fd->rf', expert_grad, down_weight, preferred_element_type=...  6.15 us
    all_gather x1, waiting for transfers between devices, per_device(): full_grad = lax.all_gather(layer_grad, 'tp', axis=1, tiled=True)  5.69 us
  transfers between devices with their start and end apart: 7, of which 6 were waited for; matrix products, arithmetic and copies ran while one was open for 31% of the time, Pallas kernels for 0%

commit v1 on v0

v1 whole, which is shorter than its diff:
```python
import functools

import jax
import jax.numpy as jnp
from jax import lax
from jax.experimental import pallas as pl
from jax.experimental.pallas import tpu as pltpu
from jax.sharding import PartitionSpec as P

clamp_limit = 7.0
swish_alpha = 1.702
F32 = jnp.float32
BF16 = jnp.bfloat16
VMEM = pl.BlockSpec(memory_space=pltpu.VMEM)
SMEM = pl.BlockSpec(memory_space=pltpu.SMEM)
params = functools.partial(pltpu.CompilerParams, vmem_limit_bytes=56 * 1024 * 1024)


def cost(flops, moved):
    return pl.CostEstimate(flops=flops, bytes_accessed=moved, transcendentals=0)


def nn(a, b):
    return lax.dot_general(a, b, (((1,), (0,)), ((), ())), preferred_element_type=F32)


def nt(a, b):
    return lax.dot_general(a, b, (((1,), (1,)), ((), ())), preferred_element_type=F32)


def tn(a, b):
    return lax.dot_general(a, b, (((0,), (0,)), ((), ())), preferred_element_type=F32)


def swapped(value, axis, step):
    count = lax.axis_size(axis)
    return lax.ppermute(value, axis, [(i, i ^ step) for i in range(count)])


def passed_along(value, axis, steps):
    count = lax.axis_size(axis)
    leading, last = (max(0, -steps), min(count, count - steps))
    return lax.ppermute(value, axis, [(source, source + steps) for source in range(leading, last)])


def gathered(shard):
    count = lax.axis_size("tp")
    found = [None] * count
    found[0] = shard
    for j in range(2, count, 2):
        found[j] = swapped(shard, "tp", j)
    for j in range(0, count, 2):
        found[j + 1] = swapped(found[j], "tp", 1)
    return found


def reorder_kernel(ids, source, target):
    target[...] = source[...]


def reordered(ids, rows, blocks):
    capacity = rows.shape[0] // blocks
    out = pl.pallas_call(
        reorder_kernel,
        grid_spec=pltpu.PrefetchScalarGridSpec(
            num_scalar_prefetch=1,
            grid=(blocks,),
            in_specs=[pl.BlockSpec((1, capacity, rows.shape[1]), lambda k, ids: (ids[0] ^ k, 0, 0))],
            out_specs=pl.BlockSpec((1, capacity, rows.shape[1]), lambda k, ids: (k, 0, 0)),
        ),
        out_shape=jax.ShapeDtypeStruct((blocks, capacity, rows.shape[1]), BF16),
        compiler_params=params(),
        cost_estimate=cost(1 << 20, 4 * rows.size),
        name="reorder",
    )(ids, rows.reshape(blocks, capacity, rows.shape[1]))
    return out.reshape(rows.shape)


def dispatch_kernel(blocks, capacity, ids, routes, weights, grads, *outs):
    chosen_out, pieces = outs[0], outs[1:]
    tokens = grads.shape[0]
    expert = ids[0] ^ lax.broadcasted_iota(jnp.int32, (blocks, tokens), 0)
    first = jnp.broadcast_to(routes[0:1, :], (blocks, tokens)) == expert
    second = jnp.broadcast_to(routes[1:2, :], (blocks, tokens)) == expert
    member = jnp.where(first | second, 1.0, 0.0)
    weight = jnp.where(first, weights[0:1, :], 0.0) + jnp.where(second, weights[1:2, :], 0.0)
    earlier = lax.broadcasted_iota(jnp.int32, (tokens, tokens), 0) < lax.broadcasted_iota(
        jnp.int32, (tokens, tokens), 1
    )
    rank = nn(member.astype(BF16), jnp.where(earlier, 1.0, 0.0).astype(BF16))
    slot = jnp.where(member > 0.5, rank, -1.0).astype(jnp.int32)
    places = lax.broadcasted_iota(jnp.int32, (capacity, tokens), 0)
    values = grads[...]
    for k in range(blocks):
        hit = jnp.broadcast_to(slot[k : k + 1, :], (capacity, tokens)) == places
        chosen = jnp.where(hit, 1.0, 0.0).astype(BF16)
        chosen_out[k] = chosen
        scale = jnp.sum(
            jnp.where(hit, jnp.broadcast_to(weight[k : k + 1, :], (capacity, tokens)), 0.0),
            axis=1,
            keepdims=True,
        )
        pieces[k][...] = (nn(chosen, values) * scale).astype(BF16)


def dispatched(ids, routes, weights, grads, blocks, capacity):
    tokens, width = grads.shape
    out = pl.pallas_call(
        functools.partial(dispatch_kernel, blocks, capacity),
        in_specs=[SMEM, VMEM, VMEM, VMEM],
        out_specs=[VMEM] * (blocks + 1),
        out_shape=[jax.ShapeDtypeStruct((blocks, capacity, tokens), BF16)]
        + [jax.ShapeDtypeStruct((capacity, width), BF16)] * blocks,
        compiler_params=params(),
        cost_estimate=cost(2 * blocks * capacity * tokens * width, 4 * blocks * capacity * width),
        name="dispatch",
    )(ids, routes.T, weights.T, grads)
    return out[0], out[1:]


def row_block(rows):
    for size in (384, 256, 192, 128, 96):
        if rows % size == 0:
            return size
    return rows


def gate_kernel(count, ids, *refs):
    saved, (w_gate, w_up, hidden, gate_factor, up_factor) = refs[:count], refs[count:]
    width = saved[0].shape[1]
    gate_pre = up_pre = 0.0
    for j in range(count):
        part = pl.ds(pl.multiple_of((ids[1] ^ j) * width, width), width)
        gate_pre += nn(saved[j][...], w_gate[part, :])
        up_pre += nn(saved[j][...], w_up[part, :])
    gate_cut = jnp.minimum(gate_pre, clamp_limit)
    up_cut = jnp.clip(up_pre, -clamp_limit, clamp_limit)
    sig = jax.nn.sigmoid(swish_alpha * gate_cut)
    swish = gate_cut * sig
    hidden[...] = ((up_cut + 1.0) * swish).astype(BF16)
    slope = sig + swish_alpha * swish * (1.0 - sig)
    gate_factor[...] = jnp.where(gate_pre < clamp_limit, (up_cut + 1.0) * slope, 0.0)
    up_factor[...] = jnp.where(jnp.abs(up_pre) < clamp_limit, swish, 0.0)


def gate_stage(ids, saved, w_gate, w_up):
    count, (rows, width) = len(saved), saved[0].shape
    units = w_gate.shape[1]
    size = row_block(rows)
    spec = pl.BlockSpec((size, width), lambda i, ids: (i, 0))
    whole = pl.BlockSpec(w_gate.shape, lambda i, ids: (0, 0))
    out = pl.BlockSpec((size, units), lambda i, ids: (i, 0))
    return pl.pallas_call(
        functools.partial(gate_kernel, count),
        grid_spec=pltpu.PrefetchScalarGridSpec(
            num_scalar_prefetch=1,
            grid=(rows // size,),
            in_specs=[spec] * count + [whole, whole],
            out_specs=[out] * 3,
        ),
        out_shape=[jax.ShapeDtypeStruct((rows, units), d) for d in (BF16, F32, F32)],
        compiler_params=params(),
        cost_estimate=cost(4 * rows * count * width * units, 8 * w_gate.size),
        name="gate_up",
    )(ids, *saved, w_gate, w_up)


def act_kernel(count, ids, *refs):
    grads = refs[:count]
    gate_factor, up_factor, w_down, w_gate, w_up, gate_grad, up_grad, sent = refs[count:]
    width = grads[0].shape[1]

    def part(j):
        return pl.ds(pl.multiple_of((ids[1] ^ j) * width, width), width)

    act = 0.0
    for j in range(count):
        act += nt(grads[j][...], w_down[:, part(j)])
    gate = (act * gate_factor[...]).astype(BF16)
    up = (act * up_factor[...]).astype(BF16)
    gate_grad[...] = gate
    up_grad[...] = up
    for j in range(1, count, 2):
        sent[j // 2] = (nt(gate, w_gate[part(j), :]) + nt(up, w_up[part(j), :])).astype(BF16)


def act_stage(ids, grads, first_row, gate_factor, up_factor, w_down, w_gate, w_up):
    count, (rows, width) = len(grads), grads[0].shape
    units = w_gate.shape[1]
    size = row_block(rows)
    first = first_row // size
    spec = pl.BlockSpec((size, width), lambda i, ids: (i, 0))
    factor = pl.BlockSpec((size, units), lambda i, ids: (i + first, 0))
    out = pl.BlockSpec((size, units), lambda i, ids: (i, 0))
    whole = pl.BlockSpec(w_gate.shape, lambda i, ids: (0, 0))
    down = pl.BlockSpec(w_down.shape, lambda i, ids: (0, 0))
    return pl.pallas_call(
        functools.partial(act_kernel, count),
        grid_spec=pltpu.PrefetchScalarGridSpec(
            num_scalar_prefetch=1,
            grid=(rows // size,),
            in_specs=[spec] * count + [factor, factor, down, whole, whole],
            out_specs=[out, out, pl.BlockSpec((count // 2, size, width), lambda i, ids: (0, i, 0))],
        ),
        out_shape=[
            jax.ShapeDtypeStruct((rows, units), BF16),
            jax.ShapeDtypeStruct((rows, units), BF16),
            jax.ShapeDtypeStruct((count // 2, rows, width), BF16),
        ],
        compiler_params=params(),
        cost_estimate=cost(4 * rows * count * width * units, 12 * w_gate.size),
        name="act",
    )(ids, *grads, gate_factor, up_factor, w_down, w_gate, w_up)


def term_kernel(pairs, ids, gate_grad, up_grad, w_gate, w_up, received, own, *sent):
    width = own.shape[1]
    for i in range(pairs):
        part = pl.ds(pl.multiple_of((ids[1] ^ (2 * i)) * width, width), width)
        term = nt(gate_grad[...], w_gate[part, :]) + nt(up_grad[...], w_up[part, :])
        total = term + received[i].astype(F32)
        if i:
            sent[i - 1][...] = total.astype(BF16)
        else:
            own[...] = total


def term_stage(ids, gate_grad, up_grad, w_gate, w_up, received):
    pairs, rows, width = received.shape
    units = w_gate.shape[1]
    size = row_block(rows)
    spec = pl.BlockSpec((size, units), lambda i, ids: (i, 0))
    whole = pl.BlockSpec(w_gate.shape, lambda i, ids: (0, 0))
    out = pl.BlockSpec((size, width), lambda i, ids: (i, 0))
    result = pl.pallas_call(
        functools.partial(term_kernel, pairs),
        grid_spec=pltpu.PrefetchScalarGridSpec(
            num_scalar_prefetch=1,
            grid=(rows // size,),
            in_specs=[spec, spec, whole, whole, pl.BlockSpec((pairs, size, width), lambda i, ids: (0, i, 0))],
            out_specs=[out] * pairs,
        ),
        out_shape=[jax.ShapeDtypeStruct((rows, width), F32)]
        + [jax.ShapeDtypeStruct((rows, width), BF16)] * (pairs - 1),
        compiler_params=params(),
        cost_estimate=cost(4 * rows * pairs * width * units, 8 * w_gate.size),
        name="terms",
    )(ids, gate_grad, up_grad, w_gate, w_up, received)
    return result[0], result[1:]


def add_kernel(count, own, *refs):
    received, outs = refs[:count], refs[count:]
    capacity = outs[0].shape[0]
    for k in range(len(outs)):
        part = pl.ds(k * capacity, capacity)
        total = own[part, :]
        for other in received:
            total += other[part, :].astype(F32)
        outs[k][...] = total.astype(BF16)


def add_stage(own, received, pieces):
    rows, width = own.shape
    return pl.pallas_call(
        functools.partial(add_kernel, len(received)),
        in_specs=[VMEM] * (1 + len(received)),
        out_specs=[VMEM] * pieces,
        out_shape=[jax.ShapeDtypeStruct((rows // pieces, width), BF16)] * pieces,
        compiler_params=params(),
        cost_estimate=cost(rows * width, 8 * rows * width),
        name="add",
    )(own, *received)


def combine_kernel(chosen, *refs):
    pieces, out = refs[:-1], refs[-1]
    total = 0.0
    for k, piece in enumerate(pieces):
        total += tn(chosen[k], piece[...])
    out[...] = total.astype(BF16)


def combined(chosen, pieces):
    tokens, width = chosen.shape[2], pieces[0].shape[1]
    return pl.pallas_call(
        combine_kernel,
        in_specs=[VMEM] * (1 + len(pieces)),
        out_specs=VMEM,
        out_shape=jax.ShapeDtypeStruct((tokens, width), BF16),
        compiler_params=params(),
        cost_estimate=cost(2 * chosen.size * width, 4 * chosen.size),
        name="combine",
    )(chosen, *pieces)


def turned_kernel(count, ids, *refs):
    saved, (gate_grad, up_grad, out_gate, out_up) = refs[:count], refs[count:]
    for j in range(count):
        @pl.when(pl.program_id(0) == j)
        def _(j=j):
            turned = saved[j][...].T
            out_gate[...] = nn(turned, gate_grad[...]).astype(BF16)
            out_up[...] = nn(turned, up_grad[...]).astype(BF16)


def in_weight_grads(ids, saved, gate_grad, up_grad):
    count, (rows, width) = len(saved), saved[0].shape
    units = gate_grad.shape[1]
    out = pl.BlockSpec((width, units), lambda j, ids: (ids[1] ^ j, 0))
    whole = pl.BlockSpec((rows, width), lambda j, ids: (0, 0))
    grad = pl.BlockSpec((rows, units), lambda j, ids: (0, 0))
    return pl.pallas_call(
        functools.partial(turned_kernel, count),
        grid_spec=pltpu.PrefetchScalarGridSpec(
            num_scalar_prefetch=1,
            grid=(count,),
            in_specs=[whole] * count + [grad, grad],
            out_specs=[out, out],
        ),
        out_shape=[jax.ShapeDtypeStruct((count * width, units), BF16)] * 2,
        compiler_params=params(),
        cost_estimate=cost(4 * rows * count * width * units, 8 * rows * width * count),
        name="in_grads",
    )(ids, *saved, gate_grad, up_grad)


def down_kernel(count, ids, *refs):
    grads, (hidden, out_down, turned) = refs[:count], refs[count:]

    @pl.when(pl.program_id(0) == 0)
    def _():
        turned[...] = hidden[...].T

    for j in range(count):
        @pl.when(pl.program_id(0) == j)
        def _(j=j):
            out_down[...] = nn(turned[...], grads[j][...]).astype(BF16)


def down_weight_grad(ids, grads, hidden):
    count, (rows, width) = len(grads), grads[0].shape
    units = hidden.shape[1]
    return pl.pallas_call(
        functools.partial(down_kernel, count),
        grid_spec=pltpu.PrefetchScalarGridSpec(
            num_scalar_prefetch=1,
            grid=(count,),
            in_specs=[pl.BlockSpec((rows, width), lambda j, ids: (0, 0))] * count
            + [pl.BlockSpec((rows, units), lambda j, ids: (0, 0))],
            out_specs=pl.BlockSpec((units, width), lambda j, ids: (0, ids[1] ^ j)),
            scratch_shapes=[pltpu.VMEM((units, rows), BF16)],
        ),
        out_shape=jax.ShapeDtypeStruct((units, count * width), BF16),
        compiler_params=params(),
        cost_estimate=cost(2 * rows * count * width * units, 4 * rows * width * count),
        name="down_grad",
    )(ids, *grads, hidden)


def mixer_kernel(count, blocks, ids, *refs):
    grads, (w_out, b_gate, conv_out, out_grad, grad_b, projected, full) = refs[:count], refs[count:]
    width = grads[0].shape[1]
    mixer = 0.0
    for j in range(count):
        part = pl.ds(pl.multiple_of((ids[1] ^ j) * width, width), width)
        mixer += nt(grads[j][...], w_out[:, part])
        full[:, part] = grads[j][...]
    gate, conv = b_gate[...].astype(F32), conv_out[...].astype(F32)
    out_grad[...] = mixer * gate
    grad_b[...] = (mixer * conv).astype(BF16)
    mixed = (gate * conv).astype(BF16).T
    if len(projected.shape) == 3:
        share = projected.shape[2]
        for k in range(blocks):
            part = pl.ds(pl.multiple_of((ids[0] ^ k) * share, share), share)
            projected[k] = nn(mixed, full[:, part]).astype(BF16)
    else:
        projected[...] = nn(mixed, full[...]).astype(BF16)


def mixer_stage(ids, grads, w_out, b_gate, conv_out, blocks):
    count, (tokens, width) = len(grads), grads[0].shape
    channels, model = w_out.shape
    share = model // blocks
    direct = share % 128 == 0
    shape = (blocks, channels, share) if direct else (channels, model)
    out_grad, grad_b, projected = pl.pallas_call(
        functools.partial(mixer_kernel, count, blocks),
        in_specs=[SMEM] + [VMEM] * (count + 3),
        out_specs=[VMEM] * 3,
        out_shape=[
            jax.ShapeDtypeStruct((tokens, channels), F32),
            jax.ShapeDtypeStruct((tokens, channels), BF16),
            jax.ShapeDtypeStruct(shape, BF16),
        ],
        scratch_shapes=[pltpu.VMEM((tokens, model), BF16)],
        compiler_params=params(),
        cost_estimate=cost(4 * tokens * channels * model, 4 * tokens * model),
        name="mixer",
    )(ids, *grads, w_out, b_gate, conv_out)
    if not direct:
        projected = projected.reshape(channels, blocks, share).transpose(1, 0, 2)
        projected = projected[jnp.arange(blocks) ^ ids[0]]
    return out_grad, grad_b, projected


def per_device(
    layer_grad,
    routes,
    route_weights,
    expert_in,
    w_gate,
    w_up,
    w_down,
    conv_in,
    c_gate,
    b_gate,
    conv_out,
    taps,
    w_out,
):
    blocks = lax.axis_size("sp")
    tok_rows = layer_grad.shape[0]
    capacity = expert_in.shape[1] // blocks
    ids = jnp.stack([lax.axis_index("sp"), lax.axis_index("tp")]).astype(jnp.int32)
    gate_weight, up_weight, down_weight = w_gate[0], w_up[0], w_down[0]

    saved = gathered(reordered(ids, expert_in[0], blocks))
    chosen, pieces = dispatched(ids, routes, route_weights, layer_grad, blocks, capacity)
    half = blocks // 2
    order = (range(half, blocks), range(half))
    arrived = [[pieces[k] if k == 0 else swapped(pieces[k], "sp", k) for k in group] for group in order]
    token_grads = gathered(layer_grad)
    expert_grads = [gathered(jnp.concatenate(group, axis=0)) for group in arrived]

    hidden, gate_factor, up_factor = gate_stage(ids, saved, gate_weight, up_weight)
    out_grad, grad_b_gate, projected = mixer_stage(ids, token_grads, w_out, b_gate, conv_out, blocks)

    gate_grads, up_grads, returned = [], [], [None] * blocks
    for group, grads in zip(order, expert_grads):
        gate_grad, up_grad, sent = act_stage(
            ids, grads, group[0] * capacity, gate_factor, up_factor, down_weight, gate_weight, up_weight
        )
        received = swapped(sent, "tp", 1)
        own, others = term_stage(ids, gate_grad, up_grad, gate_weight, up_weight, received)
        others = [swapped(value, "tp", 2 * (i + 1)) for i, value in enumerate(others)]
        for k, piece in zip(group, add_stage(own, others, len(group))):
            returned[k] = piece if k == 0 else swapped(piece, "sp", k)
        gate_grads.append(gate_grad)
        up_grads.append(up_grad)
    grad_routed = combined(chosen, returned)

    def joined(first, second):
        return jnp.concatenate([second, first], axis=0)

    grad_gate, grad_up = in_weight_grads(ids, saved, joined(*gate_grads), joined(*up_grads))
    grad_down = down_weight_grad(ids, [joined(a, b) for a, b in zip(*expert_grads)], hidden)

    while projected.shape[0] > 1:
        step = projected.shape[0] // 2
        other = swapped(projected[step:], "sp", step)
        projected = projected[:step].astype(F32) + other.astype(F32)
        if step > 1:
            projected = projected.astype(BF16)
    grad_out_proj = projected[0]

    tap_reach = taps.shape[0] - 1
    following = passed_along(out_grad[:tap_reach], "sp", -1)
    extended = jnp.concatenate([out_grad, following], axis=0)
    tap_values = taps.astype(F32)
    conv_grad = jnp.zeros_like(out_grad)
    for tap_index in range(tap_reach + 1):
        offset = tap_reach - tap_index
        conv_grad = conv_grad + tap_values[tap_index] * extended[offset : offset + tok_rows]
    grad_conv_in = (conv_grad * c_gate.astype(F32)).astype(BF16)
    grad_c_gate = (conv_grad * conv_in.astype(F32)).astype(BF16)
    return (
        grad_gate[None],
        grad_up[None],
        grad_down[None],
        grad_routed,
        grad_out_proj,
        grad_conv_in,
        grad_c_gate,
        grad_b_gate,
    )


def solution(mesh):
    in_specs = (
        P("sp", "tp"),
        P("sp", None),
        P("sp", None),
        P("sp", None, "tp"),
        P("sp", None, "tp"),
        P("sp", None, "tp"),
        P("sp", "tp", None),
        P("sp", "tp"),
        P("sp", "tp"),
        P("sp", "tp"),
        P("sp", "tp"),
        P(None, "tp"),
        P("tp", None),
    )
    out_specs = (
        P("sp", None, "tp"),
        P("sp", None, "tp"),
        P("sp", "tp", None),
        P("sp", "tp"),
        P("tp", "sp"),
        P("sp", "tp"),
        P("sp", "tp"),
        P("sp", "tp"),
    )
    return jax.shard_map(
        per_device, mesh=mesh, in_specs=in_specs, out_specs=out_specs, check_vma=False
    )
```

time: 213 us -> 166 us (0.78)
  Pallas kernels: 0 us -> 66.1 us
  waiting for transfers between devices: 96.8 us -> 38 us
  matrix products: 40.6 us -> 0 us
  starting transfers between devices: 7.3 us -> 40.3 us
  blocking collectives: 27.5 us -> 0 us
  between operations: 14 us -> 1.1 us
  local copies, waits for them, and re-layouts: 17 us -> 10.6 us
    reduce_scatter x2 -> x0, waiting for transfers between devices: 67.5 us -> none  [the longest x1 36.7 us: per_device(): lax.psum_scatter(jnp.einsum('td,tc->dc', full_grad, mixed, preferred_elem...]
    pallas_call x0 -> x13, Pallas kernels: none -> 66.1 us  [the longest x2 14.6 us: act_stage(): pl.pallas_call(functools.partial(act_kernel, count), grid_spec=pltpu.Pref...]
    dot_general x10 -> x0, matrix products: 40.6 us -> none  [the longest x1 6.18 us: per_device(): jnp.einsum('rf,rd->fd', hidden, expert_grad, preferred_element_type=jnp.f...]
    ppermute x0 -> x33, starting transfers between devices: none -> 38.8 us  [swapped(): return lax.ppermute(value, axis, [(i, i ^ step) for i in range(count)])]
    ppermute x0 -> x33, waiting for transfers between devices: none -> 35.9 us  [swapped(): return lax.ppermute(value, axis, [(i, i ^ step) for i in range(count)])]
    all_to_all x1 -> x0, blocking collectives: 27.5 us -> none  [per_device(): lax.all_to_all(buffer.reshape(sp_devices, capacity, -1), 'sp', split_axis...]
    all_gather x3 -> x0, waiting for transfers between devices: 23.8 us -> none  [the longest x1 18.1 us: per_device(): lax.all_gather(arrived.reshape(sp_devices * capacity, -1), 'tp', axis=1,...]
    all_to_all x1 -> x0, starting transfers between devices: 5.51 us -> none  [per_device(): lax.all_to_all(reduced.reshape(sp_devices, capacity, -1), 'sp', split_axi...]
  transfers between devices with their start and end apart: 7 -> 34, of which waited for: 6 -> 7; matrix products, arithmetic and copies ran while one was open for 31% -> 7% of each run, Pallas kernels for 0% -> 37%
where the time goes in v1:
time: 166 us; the launch traced here: 165 us
  Pallas kernels  66.1 us (40%)
  starting transfers between devices  40.3 us (24%)
  waiting for transfers between devices  38 us (23%)
  local copies, waits for them, and re-layouts  10.6 us (6%)
  other arithmetic  8.87 us (5%)
    ppermute x33, starting transfers between devices, swapped(): return lax.ppermute(value, axis, [(i, i ^ step) for i in range(count)])  38.8 us
    ppermute x33, waiting for transfers between devices, swapped(): return lax.ppermute(value, axis, [(i, i ^ step) for i in range(count)])  35.9 us
    pallas_call x2, Pallas kernels, act_stage(): pl.pallas_call(functools.partial(act_kernel, count), grid_spec=pltpu.Pref...  14.6 us
    pallas_call x2, Pallas kernels, term_stage(): pl.pallas_call(functools.partial(term_kernel, pairs), grid_spec=pltpu.Pre...  10.3 us
    pallas_call x1, Pallas kernels, gate_stage(): pl.pallas_call(functools.partial(gate_kernel, count), grid_spec=pltpu.Pre...  9 us
    unnamed x92, local copies, waits for them, and re-layouts  8.93 us
    pallas_call x1, Pallas kernels, in_weight_grads(): pl.pallas_call(functools.partial(turned_kernel, count), grid_spec=pltpu.P...  8.34 us
    pallas_call x1, Pallas kernels, down_weight_grad(): pl.pallas_call(functools.partial(down_kernel, count), grid_spec=pltpu.Pre...  6.18 us
  transfers between devices with their start and end apart: 34, of which 7 were waited for; matrix products, arithmetic and copies ran while one was open for 7% of the time, Pallas kernels for 37%

profile of v1, /device:TPU:0, one launch (start us, length us, event | category | flops | bytes accessed | tf_op | source)
XLA Modules:
  0.0 165.0 jit_solution(9015117784445147700)
XLA Ops:
  1.3 2.4 %dispatch.1 = (bf16[8,96,256]{2,1,0:T(8,128)(2,1)}, bf16[96,512]{1,0:T(8,128)(2,1)}, bf16[96,512]{1,0:T(8,128)(2,1)}, bf16[96,512]{1,0:T(8,128)(2,1)}, bf16[96,5...) custom-call(s32[2]{0:T(128)} %pad_add_fusion.ids, ...), custom_call_target="tpu_custom_call" | custom-call | flops 201326592 | bytes 1572864 | tf_op jit(solution)/shard_map/dispatch/pallas_call | solution.py:108
  3.7 3.0 %collective-permute-start.3 = (bf16[96,512]{1,0:T(8,128)(2,1)}, bf16[96,512]{1,0:T(8,128)(2,1)S(1)}, u32[]{:S(2)}, u32[]{:S(2)}) collective-permute-start(bf16[96,512]{1,0:T(8,128)(2,1)} %get-tuple-element.44), channel_id=1, source_target_pairs={{0,4},{4,0},{8,12},{12,8},{16,20},{20,16},{24,28},{28,24},{1,5},{5... | collective-permute-start | bytes 294920 | tf_op jit(solution)/shard_map/ppermute | solution.py:37
  8.3 3.0 %collective-permute-start.9 = (bf16[96,512]{1,0:T(8,128)(2,1)}, bf16[96,512]{1,0:T(8,128)(2,1)S(1)}, u32[]{:S(2)}, u32[]{:S(2)}) collective-permute-start(bf16[96,512]{1,0:T(8,128)(2,1)} %get-tuple-element.50), channel_id=1, source_target_pairs={{0,16},{4,20},{8,24},{12,28},{16,0},{20,4},{24,8},{28,12},{1,17},{... | collective-permute-start | bytes 294920 | tf_op jit(solution)/shard_map/ppermute | solution.py:37
  12.6 5.7 %reorder.1 = bf16[8,96,512]{2,1,0:T(8,128)(2,1)} custom-call(s32[2]{0:T(128)} %pad_add_fusion.ids, bf16[8,96,512]{2,1,0:T(8,128)(2,1)} %bitcast.33), custom_call_target="tpu_custom_call" | custom-call | flops 1048576 | bytes 1572864 | tf_op jit(solution)/shard_map/reorder/pallas_call | solution.py:63
  18.3 3.7 %collective-permute-start.11 = (bf16[96,512]{1,0:T(8,128)(2,1)S(1)}, bf16[96,512]{1,0:T(8,128)(2,1)S(1)}, u32[]{:S(2)}, u32[]{:S(2)}) collective-permute-start(bf16[96,512]{1,0:T(8,128)(2,1)S(1)} %copy-done.39), channel_id=1, source_target_pairs={{0,24},{4,28},{8,16},{12,20},{16,8},{20,12},{24,0},{28,4},{1,25},{... | collective-permute-start | bytes 294920 | tf_op jit(solution)/shard_map/ppermute | solution.py:37
  25.1 4.4 %collective-permute-done.12 = bf16[96,512]{1,0:T(8,128)(2,1)S(1)} collective-permute-done((bf16[96,512]{1,0:T(8,128)(2,1)S(1)}, bf16[96,512]{1,0:T(8,128)(2,1)S(1)}, u32[]{:S(2)}, u32[]{:S(2)}) %collective-permute-start.12) | collective-permute-done | bytes 98336 | tf_op jit(solution)/shard_map/ppermute | solution.py:37
  33.2 23.7 %collective-permute-done.28.refs_2_ = bf16[256,512]{1,0:T(8,128)(2,1)S(1)} collective-permute-done((bf16[256,512]{1,0:T(8,128)(2,1)S(1)}, bf16[256,512]{1,0:T(8,128)(2,1)S(1)}, u32[]{:S(2)}, u32[]{:S(2)}) %collective-permute-start.28) | collective-permute-done | bytes 262176 | tf_op jit(solution)/shard_map/ppermute | solution.py:37
  58.1 4.4 %collective-permute-done.7.refs_2_ = bf16[384,512]{1,0:T(8,128)(2,1)S(1)} collective-permute-done((bf16[384,512]{1,0:T(8,128)(2,1)S(1)}, bf16[384,512]{1,0:T(8,128)(2,1)S(1)}, u32[]{:S(2)}, u32[]{:S(2)}) %collective-permute-start.7) | collective-permute-done | bytes 393248 | tf_op jit(solution)/shard_map/ppermute | solution.py:37
  66.4 2.9 %mixer.1 = (f32[256,128]{1,0:T(8,128)}, bf16[256,128]{1,0:T(8,128)(2,1)}, bf16[8,128,256]{2,1,0:T(8,128)(2,1)}) custom-call(s32[2]{0:T(128)} %pad_add_fusion.ids, bf16[256,512]{1,0:T(8,128)(2,1)} %refs_0_.1, bf16[256,512]{1,0:T(8,128)(2,1)} %copy-done.22, bf16[256,512]{1,0:T(8,128)(2,1)} %copy-done.21, bf16[256,512]{1,0:T(8,128)(2,1)} %copy-done.23, ...), custom_call_target="tpu_custom_call" | custom-call | flops 268435456 | bytes 2097152 | tf_op jit(solution)/shard_map/mixer/pallas_call | solution.py:388
  73.4 2.1 %collective-permute-done.33 = f32[2,128]{1,0:T(2,128)S(1)} collective-permute-done((f32[2,128]{1,0:T(2,128)S(1)}, f32[2,128]{1,0:T(2,128)S(1)}, u32[]{:S(2)}, u32[]{:S(2)}) %collective-permute-start.33) | collective-permute-done | bytes 1056 | tf_op jit(solution)/shard_map/ppermute | solution.py:43
  78.9 9.0 %gate_up.1 = (bf16[768,512]{1,0:T(8,128)(2,1)}, f32[768,512]{1,0:T(8,128)}, f32[768,512]{1,0:T(8,128)}) custom-call(s32[2]{0:T(128)} %pad_add_fusion.ids, bf16[768,512]{1,0:T(8,128)(2,1)} %bitcast.35, bf16[768,512]{1,0:T(8,128)(2,1)} %copy-done.36, bf16[768,512]{1,0:T(8,128)(2,1)} %copy-done.35, bf16[768,512]{1,0:T(8,128)(2,1)} %copy-done.37, ...), custom_call_target="tpu_custom_call" | custom-call | flops 3221225472 | bytes 8388608 | tf_op jit(solution)/shard_map/gate_up/pallas_call | solution.py:153
  88.7 7.4 %act.3 = (bf16[384,512]{1,0:T(8,128)(2,1)}, bf16[384,512]{1,0:T(8,128)(2,1)}, bf16[2,384,512]{2,1,0:T(8,128)(2,1)}) custom-call(s32[2]{0:T(128)} %pad_add_fusion.ids, bf16[384,512]{1,0:T(8,128)(2,1)} %copy-done.16, bf16[384,512]{1,0:T(8,128)(2,1)} %copy-done.3, bf16[384,512]{1,0:T(8,128)(2,1)} %copy-done.1, bf16[384,512]{1,0:T(8,128)(2,1)} %copy-done.4, ...), custom_call_target="tpu_custom_call" | custom-call | flops 1610612736 | bytes 12582912 | tf_op jit(solution)/shard_map/act/pallas_call | solution.py:197
  97.4 7.2 %act.2 = (bf16[384,512]{1,0:T(8,128)(2,1)}, bf16[384,512]{1,0:T(8,128)(2,1)}, bf16[2,384,512]{2,1,0:T(8,128)(2,1)}) custom-call(s32[2]{0:T(128)} %pad_add_fusion.ids, bf16[384,512]{1,0:T(8,128)(2,1)} %copy-done.15, bf16[384,512]{1,0:T(8,128)(2,1)} %copy-done.2, bf16[384,512]{1,0:T(8,128)(2,1)} %copy-done, bf16[384,512]{1,0:T(8,128)(2,1)} %copy-done.6, ...), custom_call_target="tpu_custom_call" | custom-call | flops 1610612736 | bytes 12582912 | tf_op jit(solution)/shard_map/act/pallas_call | solution.py:197
  105.3 3.4 %collective-permute-start.31 = (bf16[2,128,256]{2,1,0:T(8,128)(2,1)S(1)}, bf16[2,128,256]{2,1,0:T(8,128)(2,1)S(1)}, u32[]{:S(2)}, u32[]{:S(2)}) collective-permute-start(bf16[2,128,256]{2,1,0:T(8,128)(2,1)S(1)} %slice.49), channel_id=1, source_target_pairs={{0,8},{4,12},{8,0},{12,4},{16,24},{20,28},{24,16},{28,20},{1,9},{5... | collective-permute-start | bytes 393224 | tf_op jit(solution)/shard_map/ppermute | solution.py:37
  108.7 2.0 %pad_maximum_fusion.4.refs_3_ = bf16[768,512]{1,0:T(8,128)(2,1)} fusion(bf16[384,512]{1,0:T(8,128)(2,1)S(1)} %copy-done.5, bf16[384,512]{1,0:T(8,128)(2,1)} %copy-done.6), kind=kLoop, calls=%fused_computation.4 | loop fusion | flops 1572864 | bytes 1572864 | tf_op jit(solution)/shard_map/concatenate | solution.py:455
  114.6 5.1 %terms.3 = (f32[384,512]{1,0:T(8,128)}, bf16[384,512]{1,0:T(8,128)(2,1)}) custom-call(s32[2]{0:T(128)} %pad_add_fusion.ids, bf16[384,512]{1,0:T(8,128)(2,1)} %get-tuple-element.54.gate_grad, bf16[384,512]{1,0:T(8,128)(2,1)} %get-tuple-element.56.up_grad, bf16[2048,512]{1,0:T(8,128)(2,1)} %bitcast.23, bf16[2048,512]{1,0:T(8,128)(2,1)} %bitcast.28, ...), custom_call_target="tpu_custom_call" | custom-call | flops 805306368 | bytes 8388608 | tf_op jit(solution)/shard_map/terms/pallas_call | solution.py:235
  122.7 5.2 %terms.2 = (f32[384,512]{1,0:T(8,128)}, bf16[384,512]{1,0:T(8,128)(2,1)}) custom-call(s32[2]{0:T(128)} %pad_add_fusion.ids, bf16[384,512]{1,0:T(8,128)(2,1)} %get-tuple-element.49.gate_grad, bf16[384,512]{1,0:T(8,128)(2,1)} %get-tuple-element.55.up_grad, bf16[2048,512]{1,0:T(8,128)(2,1)} %bitcast.24, bf16[2048,512]{1,0:T(8,128)(2,1)} %bitcast.29, ...), custom_call_target="tpu_custom_call" | custom-call | flops 805306368 | bytes 8388608 | tf_op jit(solution)/shard_map/terms/pallas_call | solution.py:235
  131.0 2.0 %add.34 = (bf16[96,512]{1,0:T(8,128)(2,1)}, bf16[96,512]{1,0:T(8,128)(2,1)}, bf16[96,512]{1,0:T(8,128)(2,1)}, bf16[96,512]{1,0:T(8,128)(2,1)}) custom-call(f32[384,512]{1,0:T(8,128)} %get-tuple-element.69.own, bf16[384,512]{1,0:T(8,128)(2,1)} %copy-done.19), custom_call_target="tpu_custom_call" | custom-call | flops 196608 | bytes 1572864 | tf_op jit(solution)/shard_map/add/pallas_call | solution.py:265
  136.5 8.3 %in_grads.1 = (bf16[2048,512]{1,0:T(8,128)(2,1)}, bf16[2048,512]{1,0:T(8,128)(2,1)}) custom-call(s32[2]{0:T(128)} %pad_add_fusion.ids, bf16[768,512]{1,0:T(8,128)(2,1)} %bitcast.36, bf16[768,512]{1,0:T(8,128)(2,1)} %copy-done.36, bf16[768,512]{1,0:T(8,128)(2,1)} %copy-done.35, bf16[768,512]{1,0:T(8,128)(2,1)} %copy-done.37, ...), custom_call_target="tpu_custom_call" | custom-call | flops 3221225472 | bytes 12582912 | tf_op jit(solution)/shard_map/in_grads/pallas_call | solution.py:313
  146.1 2.9 %collective-permute-start.26 = (bf16[96,512]{1,0:T(8,128)(2,1)S(1)}, bf16[96,512]{1,0:T(8,128)(2,1)S(1)}, u32[]{:S(2)}, u32[]{:S(2)}) collective-permute-start(bf16[96,512]{1,0:T(8,128)(2,1)S(1)} %copy-done.40), channel_id=1, source_target_pairs={{0,28},{4,24},{8,20},{12,16},{16,12},{20,8},{24,4},{28,0},{1,29},{... | collective-permute-start | bytes 294920 | tf_op jit(solution)/shard_map/ppermute | solution.py:37
  149.8 2.0 %add.33 = (bf16[96,512]{1,0:T(8,128)(2,1)}, bf16[96,512]{1,0:T(8,128)(2,1)}, bf16[96,512]{1,0:T(8,128)(2,1)}, bf16[96,512]{1,0:T(8,128)(2,1)}) custom-call(f32[384,512]{1,0:T(8,128)} %get-tuple-element.62.own, bf16[384,512]{1,0:T(8,128)(2,1)} %copy-done.18), custom_call_target="tpu_custom_call" | custom-call | flops 196608 | bytes 1572864 | tf_op jit(solution)/shard_map/add/pallas_call | solution.py:265
  152.9 2.4 %collective-permute-start.20 = (bf16[96,512]{1,0:T(8,128)(2,1)}, bf16[96,512]{1,0:T(8,128)(2,1)S(1)}, u32[]{:S(2)}, u32[]{:S(2)}) collective-permute-start(bf16[96,512]{1,0:T(8,128)(2,1)} %get-tuple-element.67), channel_id=1, source_target_pairs={{0,12},{4,8},{8,4},{12,0},{16,28},{20,24},{24,20},{28,16},{1,13},{... | collective-permute-start | bytes 294920 | tf_op jit(solution)/shard_map/ppermute | solution.py:37
  155.3 6.2 %down_grad.1 = bf16[512,2048]{1,0:T(8,128)(2,1)} custom-call(s32[2]{0:T(128)} %pad_add_fusion.ids, bf16[768,512]{1,0:T(8,128)(2,1)} %copy-done.11, bf16[768,512]{1,0:T(8,128)(2,1)} %pad_maximum_fusion.2.refs_1_, bf16[768,512]{1,0:T(8,128)(2,1)} %pad_maximum_fusion.3.refs_2_, bf16[768,512]{1,0:T(8,128)(2,1)} %pad_maximum_fusion.4.refs_3_, ...), custom_call_target="tpu_custom_call" | custom-call | flops 1610612736 | bytes 6291456 | tf_op jit(solution)/shard_map/down_grad/pallas_call | solution.py:344
  162.3 2.7 %combine.1 = bf16[256,512]{1,0:T(8,128)(2,1)} custom-call(bf16[8,96,256]{2,1,0:T(8,128)(2,1)} %get-tuple-element.60.chosen, bf16[96,512]{1,0:T(8,128)(2,1)} %get-tuple-element.64.refs_0_, bf16[96,512]{1,0:T(8,128)(2,1)} %copy-done.28, bf16[96,512]{1,0:T(8,128)(2,1)} %copy-done.29, bf16[96,512]{1,0:T(8,128)(2,1)} %copy-done.30, bf16[96,512]{1,0:T(8,128)(2,1)} %copy-done.24, ...), custom_call_target="tpu_custom_call" | custom-call | flops 201326592 | bytes 786432 | tf_op jit(solution)/shard_map/combine/pallas_call | solution.py:286
  (167 shorter events, 42.8 us)
Async XLA Ops:
  3.7 14.6 %collective-permute-start.3 = (bf16[96,512]{1,0:T(8,128)(2,1)}, bf16[96,512]{1,0:T(8,128)(2,1)S(1)}, u32[]{:S(2)}, u32[]{:S(2)}) collective-permute-start(bf16[96,512]{1,0:T(8,128)(2,1)} %get-tuple-element.44), channel_id=1, source_target_pairs={{0,4},{4,0},{8,12},{12,8},{16,20},{20,16},{24,28},{28,24},{1,5},{5... | collective-permute-start | bytes 294920 | tf_op jit(solution)/shard_map/ppermute | solution.py:37
  6.7 15.3 %collective-permute-start.4 = (bf16[96,512]{1,0:T(8,128)(2,1)}, bf16[96,512]{1,0:T(8,128)(2,1)S(1)}, u32[]{:S(2)}, u32[]{:S(2)}) collective-permute-start(bf16[96,512]{1,0:T(8,128)(2,1)} %get-tuple-element.45), channel_id=1, source_target_pairs={{0,8},{4,12},{8,0},{12,4},{16,24},{20,28},{24,16},{28,20},{1,9},{5... | collective-permute-start | bytes 294920 | tf_op jit(solution)/shard_map/ppermute | solution.py:37
  8.3 13.8 %collective-permute-start.5 = (bf16[96,512]{1,0:T(8,128)(2,1)}, bf16[96,512]{1,0:T(8,128)(2,1)S(1)}, u32[]{:S(2)}, u32[]{:S(2)}) collective-permute-start(bf16[96,512]{1,0:T(8,128)(2,1)} %get-tuple-element.46), channel_id=1, source_target_pairs={{0,12},{4,8},{8,4},{12,0},{16,28},{20,24},{24,20},{28,16},{1,13},{... | collective-permute-start | bytes 294920 | tf_op jit(solution)/shard_map/ppermute | solution.py:37
  8.3 15.6 %collective-permute-start.9 = (bf16[96,512]{1,0:T(8,128)(2,1)}, bf16[96,512]{1,0:T(8,128)(2,1)S(1)}, u32[]{:S(2)}, u32[]{:S(2)}) collective-permute-start(bf16[96,512]{1,0:T(8,128)(2,1)} %get-tuple-element.50), channel_id=1, source_target_pairs={{0,16},{4,20},{8,24},{12,28},{16,0},{20,4},{24,8},{28,12},{1,17},{... | collective-permute-start | bytes 294920 | tf_op jit(solution)/shard_map/ppermute | solution.py:37
  11.3 12.7 %collective-permute-start.10 = (bf16[96,512]{1,0:T(8,128)(2,1)}, bf16[96,512]{1,0:T(8,128)(2,1)S(1)}, u32[]{:S(2)}, u32[]{:S(2)}) collective-permute-start(bf16[96,512]{1,0:T(8,128)(2,1)} %get-tuple-element.51), channel_id=1, source_target_pairs={{0,20},{4,16},{8,28},{12,24},{16,4},{20,0},{24,12},{28,8},{1,21},{... | collective-permute-start | bytes 294920 | tf_op jit(solution)/shard_map/ppermute | solution.py:37
  22.2 35.3 %collective-permute-start.1 = (bf16[768,512]{1,0:T(8,128)(2,1)}, bf16[768,512]{1,0:T(8,128)(2,1)S(1)}, u32[]{:S(2)}, u32[]{:S(2)}) collective-permute-start(bf16[768,512]{1,0:T(8,128)(2,1)} %bitcast.34), channel_id=1, source_target_pairs={{0,2},{1,3},{2,0},{3,1},{4,6},{5,7},{6,4},{7,5},{8,10},{9,11},{10,... | collective-permute-start | bytes 2359304 | tf_op jit(solution)/shard_map/ppermute | solution.py:37
  29.6 27.4 %collective-permute-start.14 = (bf16[384,512]{1,0:T(8,128)(2,1)S(1)}, bf16[384,512]{1,0:T(8,128)(2,1)S(1)}, u32[]{:S(2)}, u32[]{:S(2)}) collective-permute-start(bf16[384,512]{1,0:T(8,128)(2,1)S(1)} %get-tuple-element.81.refs_0_), channel_id=1, source_target_pairs={{0,2},{1,3},{2,0},{3,1},{4,6},{5,7},{6,4},{7,5},{8,10},{9,11},{10,... | collective-permute-start | bytes 1179656 | tf_op jit(solution)/shard_map/ppermute | solution.py:37
  31.2 25.7 %collective-permute-start.28 = (bf16[256,512]{1,0:T(8,128)(2,1)S(1)}, bf16[256,512]{1,0:T(8,128)(2,1)S(1)}, u32[]{:S(2)}, u32[]{:S(2)}) collective-permute-start(bf16[256,512]{1,0:T(8,128)(2,1)S(1)} %copy-done.20), channel_id=1, source_target_pairs={{0,2},{1,3},{2,0},{3,1},{4,6},{5,7},{6,4},{7,5},{8,10},{9,11},{10,... | collective-permute-start | bytes 786440 | tf_op jit(solution)/shard_map/ppermute | solution.py:37
  31.7 26.0 %collective-permute-start.13 = (bf16[384,512]{1,0:T(8,128)(2,1)S(1)}, bf16[384,512]{1,0:T(8,128)(2,1)S(1)}, u32[]{:S(2)}, u32[]{:S(2)}) collective-permute-start(bf16[384,512]{1,0:T(8,128)(2,1)S(1)} %get-tuple-element.81.refs_0_), channel_id=1, source_target_pairs={{0,1},{1,0},{2,3},{3,2},{4,5},{5,4},{6,7},{7,6},{8,9},{9,8},{10,11... | collective-permute-start | bytes 1179656 | tf_op jit(solution)/shard_map/ppermute | solution.py:37
  31.7 30.8 %collective-permute-start.7 = (bf16[384,512]{1,0:T(8,128)(2,1)S(1)}, bf16[384,512]{1,0:T(8,128)(2,1)S(1)}, u32[]{:S(2)}, u32[]{:S(2)}) collective-permute-start(bf16[384,512]{1,0:T(8,128)(2,1)S(1)} %get-tuple-element.89.refs_0_), channel_id=1, source_target_pairs={{0,2},{1,3},{2,0},{3,1},{4,6},{5,7},{6,4},{7,5},{8,10},{9,11},{10,... | collective-permute-start | bytes 1179656 | tf_op jit(solution)/shard_map/ppermute | solution.py:37
  57.0 20.8 %collective-permute-start = (bf16[768,512]{1,0:T(8,128)(2,1)S(1)}, bf16[768,512]{1,0:T(8,128)(2,1)S(1)}, u32[]{:S(2)}, u32[]{:S(2)}) collective-permute-start(bf16[768,512]{1,0:T(8,128)(2,1)S(1)} %bitcast.37), channel_id=1, source_target_pairs={{0,1},{1,0},{2,3},{3,2},{4,5},{5,4},{6,7},{7,6},{8,9},{9,8},{10,11... | collective-permute-start | bytes 2359304 | tf_op jit(solution)/shard_map/ppermute | solution.py:37
  57.5 20.2 %collective-permute-start.2 = (bf16[768,512]{1,0:T(8,128)(2,1)S(1)}, bf16[768,512]{1,0:T(8,128)(2,1)S(1)}, u32[]{:S(2)}, u32[]{:S(2)}) collective-permute-start(bf16[768,512]{1,0:T(8,128)(2,1)S(1)} %collective-permute-done.1.refs_2_), channel_id=1, source_target_pairs={{0,1},{1,0},{2,3},{3,2},{4,5},{5,4},{6,7},{7,6},{8,9},{9,8},{10,11... | collective-permute-start | bytes 2359304 | tf_op jit(solution)/shard_map/ppermute | solution.py:37
  63.5 24.4 %collective-permute-start.15 = (bf16[384,512]{1,0:T(8,128)(2,1)S(1)}, bf16[384,512]{1,0:T(8,128)(2,1)S(1)}, u32[]{:S(2)}, u32[]{:S(2)}) collective-permute-start(bf16[384,512]{1,0:T(8,128)(2,1)S(1)} %collective-permute-done.14.refs_2_), channel_id=1, source_target_pairs={{0,1},{1,0},{2,3},{3,2},{4,5},{5,4},{6,7},{7,6},{8,9},{9,8},{10,11... | collective-permute-start | bytes 1179656 | tf_op jit(solution)/shard_map/ppermute | solution.py:37
  65.0 31.7 %collective-permute-start.8 = (bf16[384,512]{1,0:T(8,128)(2,1)S(1)}, bf16[384,512]{1,0:T(8,128)(2,1)S(1)}, u32[]{:S(2)}, u32[]{:S(2)}) collective-permute-start(bf16[384,512]{1,0:T(8,128)(2,1)S(1)} %collective-permute-done.7.refs_2_), channel_id=1, source_target_pairs={{0,1},{1,0},{2,3},{3,2},{4,5},{5,4},{6,7},{7,6},{8,9},{9,8},{10,11... | collective-permute-start | bytes 1179656 | tf_op jit(solution)/shard_map/ppermute | solution.py:37
  75.5 29.7 %collective-permute-start.30 = (bf16[4,128,256]{2,1,0:T(8,128)(2,1)S(1)}, bf16[4,128,256]{2,1,0:T(8,128)(2,1)S(1)}, u32[]{:S(2)}, u32[]{:S(2)}) collective-permute-start(bf16[4,128,256]{2,1,0:T(8,128)(2,1)S(1)} %slice.37), channel_id=1, source_target_pairs={{0,16},{4,20},{8,24},{12,28},{16,0},{20,4},{24,8},{28,12},{1,17},{... | collective-permute-start | bytes 786440 | tf_op jit(solution)/shard_map/ppermute | solution.py:37
  96.0 17.7 %collective-permute-start.21 = (bf16[2,384,512]{2,1,0:T(8,128)(2,1)}, bf16[2,384,512]{2,1,0:T(8,128)(2,1)S(1)}, u32[]{:S(2)}, u32[]{:S(2)}) collective-permute-start(bf16[2,384,512]{2,1,0:T(8,128)(2,1)} %get-tuple-element.68), channel_id=1, source_target_pairs={{0,1},{1,0},{2,3},{3,2},{4,5},{5,4},{6,7},{7,6},{8,9},{9,8},{10,11... | collective-permute-start | bytes 2359304 | tf_op jit(solution)/shard_map/ppermute | solution.py:37
  104.7 17.2 %collective-permute-start.16 = (bf16[2,384,512]{2,1,0:T(8,128)(2,1)}, bf16[2,384,512]{2,1,0:T(8,128)(2,1)S(1)}, u32[]{:S(2)}, u32[]{:S(2)}) collective-permute-start(bf16[2,384,512]{2,1,0:T(8,128)(2,1)} %get-tuple-element.61), channel_id=1, source_target_pairs={{0,1},{1,0},{2,3},{3,2},{4,5},{5,4},{6,7},{7,6},{8,9},{9,8},{10,11... | collective-permute-start | bytes 2359304 | tf_op jit(solution)/shard_map/ppermute | solution.py:37
  119.6 10.6 %collective-permute-start.22 = (bf16[384,512]{1,0:T(8,128)(2,1)}, bf16[384,512]{1,0:T(8,128)(2,1)S(1)}, u32[]{:S(2)}, u32[]{:S(2)}) collective-permute-start(bf16[384,512]{1,0:T(8,128)(2,1)} %get-tuple-element.70), channel_id=1, source_target_pairs={{0,2},{1,3},{2,0},{3,1},{4,6},{5,7},{6,4},{7,5},{8,10},{9,11},{10,... | collective-permute-start | bytes 1179656 | tf_op jit(solution)/shard_map/ppermute | solution.py:37
  127.9 21.1 %collective-permute-start.17 = (bf16[384,512]{1,0:T(8,128)(2,1)}, bf16[384,512]{1,0:T(8,128)(2,1)S(1)}, u32[]{:S(2)}, u32[]{:S(2)}) collective-permute-start(bf16[384,512]{1,0:T(8,128)(2,1)} %get-tuple-element.63), channel_id=1, source_target_pairs={{0,2},{1,3},{2,0},{3,1},{4,6},{5,7},{6,4},{7,5},{8,10},{9,11},{10,... | collective-permute-start | bytes 1179656 | tf_op jit(solution)/shard_map/ppermute | solution.py:37
  133.0 19.9 %collective-permute-start.23 = (bf16[96,512]{1,0:T(8,128)(2,1)}, bf16[96,512]{1,0:T(8,128)(2,1)S(1)}, u32[]{:S(2)}, u32[]{:S(2)}) collective-permute-start(bf16[96,512]{1,0:T(8,128)(2,1)} %get-tuple-element.71), channel_id=1, source_target_pairs={{0,16},{4,20},{8,24},{12,28},{16,0},{20,4},{24,8},{28,12},{1,17},{... | collective-permute-start | bytes 294920 | tf_op jit(solution)/shard_map/ppermute | solution.py:37
  134.8 18.1 %collective-permute-start.24 = (bf16[96,512]{1,0:T(8,128)(2,1)}, bf16[96,512]{1,0:T(8,128)(2,1)S(1)}, u32[]{:S(2)}, u32[]{:S(2)}) collective-permute-start(bf16[96,512]{1,0:T(8,128)(2,1)} %get-tuple-element.72), channel_id=1, source_target_pairs={{0,20},{4,16},{8,28},{12,24},{16,4},{20,0},{24,12},{28,8},{1,21},{... | collective-permute-start | bytes 294920 | tf_op jit(solution)/shard_map/ppermute | solution.py:37
  144.8 16.6 %collective-permute-start.25 = (bf16[96,512]{1,0:T(8,128)(2,1)S(1)}, bf16[96,512]{1,0:T(8,128)(2,1)S(1)}, u32[]{:S(2)}, u32[]{:S(2)}) collective-permute-start(bf16[96,512]{1,0:T(8,128)(2,1)S(1)} %copy-done.41), channel_id=1, source_target_pairs={{0,24},{4,28},{8,16},{12,20},{16,8},{20,12},{24,0},{28,4},{1,25},{... | collective-permute-start | bytes 294920 | tf_op jit(solution)/shard_map/ppermute | solution.py:37
  146.1 15.3 %collective-permute-start.26 = (bf16[96,512]{1,0:T(8,128)(2,1)S(1)}, bf16[96,512]{1,0:T(8,128)(2,1)S(1)}, u32[]{:S(2)}, u32[]{:S(2)}) collective-permute-start(bf16[96,512]{1,0:T(8,128)(2,1)S(1)} %copy-done.40), channel_id=1, source_target_pairs={{0,28},{4,24},{8,20},{12,16},{16,12},{20,8},{24,4},{28,0},{1,29},{... | collective-permute-start | bytes 294920 | tf_op jit(solution)/shard_map/ppermute | solution.py:37
  151.7 9.7 %collective-permute-start.18 = (bf16[96,512]{1,0:T(8,128)(2,1)}, bf16[96,512]{1,0:T(8,128)(2,1)S(1)}, u32[]{:S(2)}, u32[]{:S(2)}) collective-permute-start(bf16[96,512]{1,0:T(8,128)(2,1)} %get-tuple-element.65), channel_id=1, source_target_pairs={{0,4},{4,0},{8,12},{12,8},{16,20},{20,16},{24,28},{28,24},{1,5},{5... | collective-permute-start | bytes 294920 | tf_op jit(solution)/shard_map/ppermute | solution.py:37
  (52 other events, 479.6 us)

commit v2 on v1

--- a/solution.py
+++ b/solution.py
@@ -13,7 +13,10 @@
 BF16 = jnp.bfloat16
 VMEM = pl.BlockSpec(memory_space=pltpu.VMEM)
 SMEM = pl.BlockSpec(memory_space=pltpu.SMEM)
-params = functools.partial(pltpu.CompilerParams, vmem_limit_bytes=56 * 1024 * 1024)
+
+
+def params(mebibytes):
+    return pltpu.CompilerParams(vmem_limit_bytes=mebibytes * 1024 * 1024)
 
 
 def cost(flops, moved):
@@ -69,7 +72,7 @@
             out_specs=pl.BlockSpec((1, capacity, rows.shape[1]), lambda k, ids: (k, 0, 0)),
         ),
         out_shape=jax.ShapeDtypeStruct((blocks, capacity, rows.shape[1]), BF16),
-        compiler_params=params(),
+        compiler_params=params(8),
         cost_estimate=cost(1 << 20, 4 * rows.size),
         name="reorder",
     )(ids, rows.reshape(blocks, capacity, rows.shape[1]))
@@ -111,7 +114,7 @@
         out_specs=[VMEM] * (blocks + 1),
         out_shape=[jax.ShapeDtypeStruct((blocks, capacity, tokens), BF16)]
         + [jax.ShapeDtypeStruct((capacity, width), BF16)] * blocks,
-        compiler_params=params(),
+        compiler_params=params(16),
         cost_estimate=cost(2 * blocks * capacity * tokens * width, 4 * blocks * capacity * width),
         name="dispatch",
     )(ids, routes.T, weights.T, grads)
@@ -125,89 +128,91 @@
     return rows
 
 
-def gate_kernel(count, ids, *refs):
+def part_of(ids, j, width):
+    return pl.ds(pl.multiple_of((ids[1] ^ j) * width, width), width)
+
+
+def block_of(ids, k, capacity):
+    return pl.ds(pl.multiple_of((ids[0] ^ k) * capacity, capacity), capacity)
+
+
+def gate_kernel(count, blocks, ids, *refs):
     saved, (w_gate, w_up, hidden, gate_factor, up_factor) = refs[:count], refs[count:]
-    width = saved[0].shape[1]
-    gate_pre = up_pre = 0.0
-    for j in range(count):
-        part = pl.ds(pl.multiple_of((ids[1] ^ j) * width, width), width)
-        gate_pre += nn(saved[j][...], w_gate[part, :])
-        up_pre += nn(saved[j][...], w_up[part, :])
-    gate_cut = jnp.minimum(gate_pre, clamp_limit)
-    up_cut = jnp.clip(up_pre, -clamp_limit, clamp_limit)
-    sig = jax.nn.sigmoid(swish_alpha * gate_cut)
-    swish = gate_cut * sig
-    hidden[...] = ((up_cut + 1.0) * swish).astype(BF16)
-    slope = sig + swish_alpha * swish * (1.0 - sig)
-    gate_factor[...] = jnp.where(gate_pre < clamp_limit, (up_cut + 1.0) * slope, 0.0)
-    up_factor[...] = jnp.where(jnp.abs(up_pre) < clamp_limit, swish, 0.0)
-
-
-def gate_stage(ids, saved, w_gate, w_up):
+    rows, width = saved[0].shape
+    capacity = rows // blocks if blocks else rows
+    parts = [part_of(ids, j, width) for j in range(count)]
+    size = row_block(rows)
+    for begin in range(0, rows, size):
+        here = pl.ds(begin, size)
+        values = jnp.concatenate([ref[here, :] for ref in saved], axis=1)
+        gate_pre = nn(values, jnp.concatenate([w_gate[part, :] for part in parts], axis=0))
+        up_pre = nn(values, jnp.concatenate([w_up[part, :] for part in parts], axis=0))
+        gate_cut = jnp.minimum(gate_pre, clamp_limit)
+        up_cut = jnp.clip(up_pre, -clamp_limit, clamp_limit)
+        sig = jax.nn.sigmoid(swish_alpha * gate_cut)
+        swish = gate_cut * sig
+        slope = sig + swish_alpha * swish * (1.0 - sig)
+        results = (
+            (hidden, ((up_cut + 1.0) * swish).astype(BF16)),
+            (gate_factor, jnp.where(gate_pre < clamp_limit, (up_cut + 1.0) * slope, 0.0)),
+            (up_factor, jnp.where(jnp.abs(up_pre) < clamp_limit, swish, 0.0)),
+        )
+        for ref, value in results:
+            if not blocks:
+                ref[here, :] = value
+                continue
+            for low in range(0, size, capacity):
+                place = block_of(ids, (begin + low) // capacity, capacity)
+                ref[place, :] = value[low : low + capacity, :]
+
+
+def gate_stage(ids, saved, w_gate, w_up, blocks):
     count, (rows, width) = len(saved), saved[0].shape
     units = w_gate.shape[1]
-    size = row_block(rows)
-    spec = pl.BlockSpec((size, width), lambda i, ids: (i, 0))
-    whole = pl.BlockSpec(w_gate.shape, lambda i, ids: (0, 0))
-    out = pl.BlockSpec((size, units), lambda i, ids: (i, 0))
     return pl.pallas_call(
-        functools.partial(gate_kernel, count),
-        grid_spec=pltpu.PrefetchScalarGridSpec(
-            num_scalar_prefetch=1,
-            grid=(rows // size,),
-            in_specs=[spec] * count + [whole, whole],
-            out_specs=[out] * 3,
-        ),
+        functools.partial(gate_kernel, count, blocks),
+        in_specs=[SMEM] + [VMEM] * (count + 2),
+        out_specs=[VMEM] * 3,
         out_shape=[jax.ShapeDtypeStruct((rows, units), d) for d in (BF16, F32, F32)],
-        compiler_params=params(),
+        compiler_params=params(16),
         cost_estimate=cost(4 * rows * count * width * units, 8 * w_gate.size),
         name="gate_up",
     )(ids, *saved, w_gate, w_up)
 
 
-def act_kernel(count, ids, *refs):
+def act_kernel(count, first, ids, *refs):
     grads = refs[:count]
     gate_factor, up_factor, w_down, w_gate, w_up, gate_grad, up_grad, sent = refs[count:]
-    width = grads[0].shape[1]
-
-    def part(j):
-        return pl.ds(pl.multiple_of((ids[1] ^ j) * width, width), width)
-
-    act = 0.0
-    for j in range(count):
-        act += nt(grads[j][...], w_down[:, part(j)])
-    gate = (act * gate_factor[...]).astype(BF16)
-    up = (act * up_factor[...]).astype(BF16)
+    rows, width = grads[0].shape
+    parts = [part_of(ids, j, width) for j in range(count)]
+    here = pl.ds(first, rows)
+    act = nt(
+        jnp.concatenate([ref[...] for ref in grads], axis=1),
+        jnp.concatenate([w_down[:, part] for part in parts], axis=1),
+    )
+    gate = (act * gate_factor[here, :]).astype(BF16)
+    up = (act * up_factor[here, :]).astype(BF16)
     gate_grad[...] = gate
     up_grad[...] = up
+    both = jnp.concatenate([gate, up], axis=1)
     for j in range(1, count, 2):
-        sent[j // 2] = (nt(gate, w_gate[part(j), :]) + nt(up, w_up[part(j), :])).astype(BF16)
-
-
-def act_stage(ids, grads, first_row, gate_factor, up_factor, w_down, w_gate, w_up):
+        weights = jnp.concatenate([w_gate[parts[j], :], w_up[parts[j], :]], axis=1)
+        sent[j // 2] = nt(both, weights).astype(BF16)
+
+
+def act_stage(ids, grads, first, gate_factor, up_factor, w_down, w_gate, w_up):
     count, (rows, width) = len(grads), grads[0].shape
     units = w_gate.shape[1]
-    size = row_block(rows)
-    first = first_row // size
-    spec = pl.BlockSpec((size, width), lambda i, ids: (i, 0))
-    factor = pl.BlockSpec((size, units), lambda i, ids: (i + first, 0))
-    out = pl.BlockSpec((size, units), lambda i, ids: (i, 0))
-    whole = pl.BlockSpec(w_gate.shape, lambda i, ids: (0, 0))
-    down = pl.BlockSpec(w_down.shape, lambda i, ids: (0, 0))
     return pl.pallas_call(
-        functools.partial(act_kernel, count),
-        grid_spec=pltpu.PrefetchScalarGridSpec(
-            num_scalar_prefetch=1,
-            grid=(rows // size,),
-            in_specs=[spec] * count + [factor, factor, down, whole, whole],
-            out_specs=[out, out, pl.BlockSpec((count // 2, size, width), lambda i, ids: (0, i, 0))],
-        ),
+        functools.partial(act_kernel, count, first),
+        in_specs=[SMEM] + [VMEM] * (count + 5),
+        out_specs=[VMEM] * 3,
         out_shape=[
             jax.ShapeDtypeStruct((rows, units), BF16),
             jax.ShapeDtypeStruct((rows, units), BF16),
             jax.ShapeDtypeStruct((count // 2, rows, width), BF16),
         ],
-        compiler_params=params(),
+        compiler_params=params(12),
         cost_estimate=cost(4 * rows * count * width * units, 12 * w_gate.size),
         name="act",
     )(ids, *grads, gate_factor, up_factor, w_down, w_gate, w_up)
@@ -215,10 +220,11 @@
 
 def term_kernel(pairs, ids, gate_grad, up_grad, w_gate, w_up, received, own, *sent):
     width = own.shape[1]
-    for i in range(pairs):
-        part = pl.ds(pl.multiple_of((ids[1] ^ (2 * i)) * width, width), width)
-        term = nt(gate_grad[...], w_gate[part, :]) + nt(up_grad[...], w_up[part, :])
-        total = term + received[i].astype(F32)
+    both = jnp.concatenate([gate_grad[...], up_grad[...]], axis=1)
+    for i in reversed(range(pairs)):
+        part = part_of(ids, 2 * i, width)
+        weights = jnp.concatenate([w_gate[part, :], w_up[part, :]], axis=1)
+        total = nt(both, weights) + received[i].astype(F32)
         if i:
             sent[i - 1][...] = total.astype(BF16)
         else:
@@ -228,26 +234,17 @@
 def term_stage(ids, gate_grad, up_grad, w_gate, w_up, received):
     pairs, rows, width = received.shape
     units = w_gate.shape[1]
-    size = row_block(rows)
-    spec = pl.BlockSpec((size, units), lambda i, ids: (i, 0))
-    whole = pl.BlockSpec(w_gate.shape, lambda i, ids: (0, 0))
-    out = pl.BlockSpec((size, width), lambda i, ids: (i, 0))
     result = pl.pallas_call(
         functools.partial(term_kernel, pairs),
-        grid_spec=pltpu.PrefetchScalarGridSpec(
-            num_scalar_prefetch=1,
-            grid=(rows // size,),
-            in_specs=[spec, spec, whole, whole, pl.BlockSpec((pairs, size, width), lambda i, ids: (0, i, 0))],
-            out_specs=[out] * pairs,
-        ),
+        in_specs=[SMEM] + [VMEM] * 5,
+        out_specs=[VMEM] * pairs,
         out_shape=[jax.ShapeDtypeStruct((rows, width), F32)]
         + [jax.ShapeDtypeStruct((rows, width), BF16)] * (pairs - 1),
-        compiler_params=params(),
+        compiler_params=params(12),
         cost_estimate=cost(4 * rows * pairs * width * units, 8 * w_gate.size),
         name="terms",
     )(ids, gate_grad, up_grad, w_gate, w_up, received)
     return result[0], result[1:]
-
 
 def add_kernel(count, own, *refs):
     received, outs = refs[:count], refs[count:]
@@ -267,7 +264,7 @@
         in_specs=[VMEM] * (1 + len(received)),
         out_specs=[VMEM] * pieces,
         out_shape=[jax.ShapeDtypeStruct((rows // pieces, width), BF16)] * pieces,
-        compiler_params=params(),
+        compiler_params=params(8),
         cost_estimate=cost(rows * width, 8 * rows * width),
         name="add",
     )(own, *received)
@@ -288,74 +285,75 @@
         in_specs=[VMEM] * (1 + len(pieces)),
         out_specs=VMEM,
         out_shape=jax.ShapeDtypeStruct((tokens, width), BF16),
-        compiler_params=params(),
+        compiler_params=params(8),
         cost_estimate=cost(2 * chosen.size * width, 4 * chosen.size),
         name="combine",
     )(chosen, *pieces)
 
 
-def turned_kernel(count, ids, *refs):
-    saved, (gate_grad, up_grad, out_gate, out_up) = refs[:count], refs[count:]
+def weight_kernel(count, blocks, ids, *refs):
+    saved, refs = refs[:count], refs[count:]
+    grads, refs = refs[: 2 * count], refs[2 * count :]
+    hidden, gates, ups = refs[0], refs[1:3], refs[3:5]
+    out_gate, out_up, out_down, both, turned, tiles, downs, sems = refs[5:]
+    rows, width = saved[0].shape
+    units = hidden.shape[1]
+    low = gates[1].shape[0]
+    copies = []
+
+    def leave(tile, target):
+        copies.append(pltpu.make_async_copy(tile, target, sems.at[len(copies)]))
+        copies[-1].start()
+
+    turned[...] = hidden[...].T
     for j in range(count):
-        @pl.when(pl.program_id(0) == j)
-        def _(j=j):
-            turned = saved[j][...].T
-            out_gate[...] = nn(turned, gate_grad[...]).astype(BF16)
-            out_up[...] = nn(turned, up_grad[...]).astype(BF16)
-
-
-def in_weight_grads(ids, saved, gate_grad, up_grad):
+        part = part_of(ids, j, width)
+        downs[j] = (
+            nn(turned[:, low:], grads[j][...]) + nn(turned[:, :low], grads[count + j][...])
+        ).astype(BF16)
+        leave(downs.at[j], out_down.at[:, part])
+    capacity = rows // blocks if blocks else rows
+    for side, pair in enumerate((gates, ups)):
+        column = slice(side * units, (side + 1) * units)
+        for ref, first in zip(pair, (low, 0)):
+            if not blocks:
+                both[first : first + ref.shape[0], column] = ref[...]
+                continue
+            for begin in range(0, ref.shape[0], capacity):
+                place = block_of(ids, (first + begin) // capacity, capacity)
+                both[place, column] = ref[begin : begin + capacity, :]
+    for j in range(count):
+        part = part_of(ids, j, width)
+        result = nn(saved[j][...].T, both[...]).astype(BF16)
+        tiles[j, 0] = result[:, :units]
+        tiles[j, 1] = result[:, units:]
+        leave(tiles.at[j, 0], out_gate.at[part, :])
+        leave(tiles.at[j, 1], out_up.at[part, :])
+    for copy in copies:
+        copy.wait()
+
+
+def weight_grads(ids, saved, grads, hidden, gate_grads, up_grads, blocks):
     count, (rows, width) = len(saved), saved[0].shape
-    units = gate_grad.shape[1]
-    out = pl.BlockSpec((width, units), lambda j, ids: (ids[1] ^ j, 0))
-    whole = pl.BlockSpec((rows, width), lambda j, ids: (0, 0))
-    grad = pl.BlockSpec((rows, units), lambda j, ids: (0, 0))
+    units = hidden.shape[1]
+    anywhere = pl.BlockSpec(memory_space=pl.ANY)
+    model = count * width
     return pl.pallas_call(
-        functools.partial(turned_kernel, count),
-        grid_spec=pltpu.PrefetchScalarGridSpec(
-            num_scalar_prefetch=1,
-            grid=(count,),
-            in_specs=[whole] * count + [grad, grad],
-            out_specs=[out, out],
-        ),
-        out_shape=[jax.ShapeDtypeStruct((count * width, units), BF16)] * 2,
-        compiler_params=params(),
-        cost_estimate=cost(4 * rows * count * width * units, 8 * rows * width * count),
-        name="in_grads",
-    )(ids, *saved, gate_grad, up_grad)
-
-
-def down_kernel(count, ids, *refs):
-    grads, (hidden, out_down, turned) = refs[:count], refs[count:]
-
-    @pl.when(pl.program_id(0) == 0)
-    def _():
-        turned[...] = hidden[...].T
-
-    for j in range(count):
-        @pl.when(pl.program_id(0) == j)
-        def _(j=j):
-            out_down[...] = nn(turned[...], grads[j][...]).astype(BF16)
-
-
-def down_weight_grad(ids, grads, hidden):
-    count, (rows, width) = len(grads), grads[0].shape
-    units = hidden.shape[1]
-    return pl.pallas_call(
-        functools.partial(down_kernel, count),
-        grid_spec=pltpu.PrefetchScalarGridSpec(
-            num_scalar_prefetch=1,
-            grid=(count,),
-            in_specs=[pl.BlockSpec((rows, width), lambda j, ids: (0, 0))] * count
-            + [pl.BlockSpec((rows, units), lambda j, ids: (0, 0))],
-            out_specs=pl.BlockSpec((units, width), lambda j, ids: (0, ids[1] ^ j)),
-            scratch_shapes=[pltpu.VMEM((units, rows), BF16)],
-        ),
-        out_shape=jax.ShapeDtypeStruct((units, count * width), BF16),
-        compiler_params=params(),
-        cost_estimate=cost(2 * rows * count * width * units, 4 * rows * width * count),
-        name="down_grad",
-    )(ids, *grads, hidden)
+        functools.partial(weight_kernel, count, blocks),
+        in_specs=[SMEM] + [VMEM] * (3 * count + 5),
+        out_specs=[anywhere] * 3,
+        out_shape=[jax.ShapeDtypeStruct(s, BF16) for s in ((model, units), (model, units), (units, model))],
+        scratch_shapes=[
+            pltpu.VMEM((rows, 2 * units), BF16),
+            pltpu.VMEM((units, rows), BF16),
+            pltpu.VMEM((count, 2, width, units), BF16),
+            pltpu.VMEM((count, units, width), BF16),
+            pltpu.SemaphoreType.DMA((3 * count,)),
+        ],
+        compiler_params=params(24),
+        cost_estimate=cost(6 * rows * model * units, 12 * rows * model),
+        name="weight_grads",
+    )(ids, *saved, *grads[0], *grads[1], hidden, *gate_grads, *up_grads)
 
 
 def mixer_kernel(count, blocks, ids, *refs):
@@ -395,7 +393,7 @@
             jax.ShapeDtypeStruct(shape, BF16),
         ],
         scratch_shapes=[pltpu.VMEM((tokens, model), BF16)],
-        compiler_params=params(),
+        compiler_params=params(16),
         cost_estimate=cost(4 * tokens * channels * model, 4 * tokens * model),
         name="mixer",
     )(ids, *grads, w_out, b_gate, conv_out)
@@ -426,7 +424,9 @@
     ids = jnp.stack([lax.axis_index("sp"), lax.axis_index("tp")]).astype(jnp.int32)
     gate_weight, up_weight, down_weight = w_gate[0], w_up[0], w_down[0]
 
-    saved = gathered(reordered(ids, expert_in[0], blocks))
+    inside = blocks if capacity % 16 == 0 else 0
+    rows = expert_in[0] if inside else reordered(ids, expert_in[0], blocks)
+    saved = gathered(rows)
     chosen, pieces = dispatched(ids, routes, route_weights, layer_grad, blocks, capacity)
     half = blocks // 2
     order = (range(half, blocks), range(half))
@@ -434,7 +434,7 @@
     token_grads = gathered(layer_grad)
     expert_grads = [gathered(jnp.concatenate(group, axis=0)) for group in arrived]
 
-    hidden, gate_factor, up_factor = gate_stage(ids, saved, gate_weight, up_weight)
+    hidden, gate_factor, up_factor = gate_stage(ids, saved, gate_weight, up_weight, inside)
     out_grad, grad_b_gate, projected = mixer_stage(ids, token_grads, w_out, b_gate, conv_out, blocks)
 
     gate_grads, up_grads, returned = [], [], [None] * blocks
@@ -451,11 +451,9 @@
         up_grads.append(up_grad)
     grad_routed = combined(chosen, returned)
 
-    def joined(first, second):
-        return jnp.concatenate([second, first], axis=0)
-
-    grad_gate, grad_up = in_weight_grads(ids, saved, joined(*gate_grads), joined(*up_grads))
-    grad_down = down_weight_grad(ids, [joined(a, b) for a, b in zip(*expert_grads)], hidden)
+    grad_gate, grad_up, grad_down = weight_grads(
+        ids, saved, expert_grads, hidden, gate_grads, up_grads, inside
+    )
 
     while projected.shape[0] > 1:
         step = projected.shape[0] // 2

time: 166 us -> 126 us (0.76)
  Pallas kernels: 66.1 us -> 26.3 us
  waiting for transfers between devices: 38 us -> 45.4 us
  other arithmetic: 8.87 us -> 2.86 us
  local copies, waits for them, and re-layouts: 10.6 us -> 7.81 us
  starting transfers between devices: 40.3 us -> 42.4 us
    pallas_call x8 -> x6, Pallas kernels: 54.1 us -> 21.6 us  [the longest x1 8.13 us: weight_grads(): pl.pallas_call(functools.partial(weight_kernel, count, blocks), in_specs=...]
    ppermute x33, waiting for transfers between devices: 35.9 us -> 45.4 us  [swapped(): return lax.ppermute(value, axis, [(i, i ^ step) for i in range(count)])]
    concatenate x4 -> x0, other arithmetic: 5.21 us -> none  [joined(): return jnp.concatenate([second, first], axis=0)]
    pallas_call x2, Pallas kernels: 3.97 us -> 0.13 us  [add_stage(): pl.pallas_call(functools.partial(add_kernel, len(received)), in_specs=[VM...]
    ppermute x33, starting transfers between devices: 38.8 us -> 41 us  [swapped(): return lax.ppermute(value, axis, [(i, i ^ step) for i in range(count)])]
    ppermute x1, waiting for transfers between devices: 2.1 us -> 0.01 us  [passed_along(): lax.ppermute(value, axis, [(source, source + steps) for source in range(l...]
    unnamed x92 -> x37, local copies, waits for them, and re-layouts: 8.93 us -> 7.74 us
  transfers between devices with their start and end apart: 34 -> 34, of which waited for: 7 -> 13; matrix products, arithmetic and copies ran while one was open for 7% -> 2% of each run, Pallas kernels for 37% -> 20%
where the time goes in v2:
time: 126 us
  waiting for transfers between devices  45.4 us (36%)
  starting transfers between devices  42.4 us (34%)
  Pallas kernels  26.3 us (21%)
  local copies, waits for them, and re-layouts  7.81 us (6%)
  other arithmetic  2.86 us (2%)
    ppermute x33, waiting for transfers between devices, swapped(): return lax.ppermute(value, axis, [(i, i ^ step) for i in range(count)])  45.4 us
    ppermute x33, starting transfers between devices, swapped(): return lax.ppermute(value, axis, [(i, i ^ step) for i in range(count)])  41 us
    pallas_call x1, Pallas kernels, weight_grads(): pl.pallas_call(functools.partial(weight_kernel, count, blocks), in_specs=...  8.13 us
    unnamed x37, local copies, waits for them, and re-layouts  7.74 us
    pallas_call x1, Pallas kernels, gate_stage(): pl.pallas_call(functools.partial(gate_kernel, count, blocks), in_specs=[S...  5.46 us
    pallas_call x2, Pallas kernels, act_stage(): pl.pallas_call(functools.partial(act_kernel, count, first), in_specs=[SME...  4.91 us
    pallas_call x2, Pallas kernels, term_stage(): pl.pallas_call(functools.partial(term_kernel, pairs), in_specs=[SMEM] + [...  3.12 us
  transfers between devices with their start and end apart: 34, of which 13 were waited for; matrix products, arithmetic and copies ran while one was open for 2% of the time, Pallas kernels for 20%

profile of v2, /device:TPU:0, one launch (start us, length us, event | category | flops | bytes accessed | tf_op | source)
XLA Modules:
  0.0 125.7 jit_solution(7956145911355509684)
XLA Ops:
  0.7 3.1 %collective-permute-start.1 = (bf16[768,512]{1,0:T(8,128)(2,1)}, bf16[768,512]{1,0:T(8,128)(2,1)}, u32[]{:S(2)}, u32[]{:S(2)}) collective-permute-start(bf16[768,512]{1,0:T(8,128)(2,1)} %bitcast.31), channel_id=1, source_target_pairs={{0,2},{1,3},{2,0},{3,1},{4,6},{5,7},{6,4},{7,5},{8,10},{9,11},{10,... | collective-permute-start | bytes 2359304 | tf_op jit(solution)/shard_map/ppermute | solution.py:40
  7.5 3.0 %collective-permute-start.3 = (bf16[96,512]{1,0:T(8,128)(2,1)S(1)}, bf16[96,512]{1,0:T(8,128)(2,1)S(1)}, u32[]{:S(2)}, u32[]{:S(2)}) collective-permute-start(bf16[96,512]{1,0:T(8,128)(2,1)S(1)} %get-tuple-element.44), channel_id=1, source_target_pairs={{0,16},{4,20},{8,24},{12,28},{16,0},{20,4},{24,8},{28,12},{1,17},{... | collective-permute-start | bytes 294920 | tf_op jit(solution)/shard_map/ppermute | solution.py:40
  11.8 6.6 %collective-permute-done.3 = bf16[96,512]{1,0:T(8,128)(2,1)S(1)} collective-permute-done((bf16[96,512]{1,0:T(8,128)(2,1)S(1)}, bf16[96,512]{1,0:T(8,128)(2,1)S(1)}, u32[]{:S(2)}, u32[]{:S(2)}) %collective-permute-start.3) | collective-permute-done | bytes 98336 | tf_op jit(solution)/shard_map/ppermute | solution.py:40
  18.4 3.1 %collective-permute-start.5 = (bf16[96,512]{1,0:T(8,128)(2,1)S(1)}, bf16[96,512]{1,0:T(8,128)(2,1)S(1)}, u32[]{:S(2)}, u32[]{:S(2)}) collective-permute-start(bf16[96,512]{1,0:T(8,128)(2,1)S(1)} %get-tuple-element.46), channel_id=1, source_target_pairs={{0,24},{4,28},{8,16},{12,20},{16,8},{20,12},{24,0},{28,4},{1,25},{... | collective-permute-start | bytes 294920 | tf_op jit(solution)/shard_map/ppermute | solution.py:40
  21.5 3.0 %collective-permute-start.6 = (bf16[96,512]{1,0:T(8,128)(2,1)S(1)}, bf16[96,512]{1,0:T(8,128)(2,1)S(1)}, u32[]{:S(2)}, u32[]{:S(2)}) collective-permute-start(bf16[96,512]{1,0:T(8,128)(2,1)S(1)} %get-tuple-element.47), channel_id=1, source_target_pairs={{0,28},{4,24},{8,20},{12,16},{16,12},{20,8},{24,4},{28,0},{1,29},{... | collective-permute-start | bytes 294920 | tf_op jit(solution)/shard_map/ppermute | solution.py:40
  24.8 1.9 %collective-permute-start.10 = (bf16[96,512]{1,0:T(8,128)(2,1)S(1)}, bf16[96,512]{1,0:T(8,128)(2,1)S(1)}, u32[]{:S(2)}, u32[]{:S(2)}) collective-permute-start(bf16[96,512]{1,0:T(8,128)(2,1)S(1)} %get-tuple-element.49), channel_id=1, source_target_pairs={{0,4},{4,0},{8,12},{12,8},{16,20},{20,16},{24,28},{28,24},{1,5},{5... | collective-permute-start | bytes 294920 | tf_op jit(solution)/shard_map/ppermute | solution.py:40
  26.7 2.2 %collective-permute-done.6 = bf16[96,512]{1,0:T(8,128)(2,1)S(1)} collective-permute-done((bf16[96,512]{1,0:T(8,128)(2,1)S(1)}, bf16[96,512]{1,0:T(8,128)(2,1)S(1)}, u32[]{:S(2)}, u32[]{:S(2)}) %collective-permute-start.6) | collective-permute-done | bytes 98336 | tf_op jit(solution)/shard_map/ppermute | solution.py:40
  28.9 1.8 %collective-permute-start.11 = (bf16[96,512]{1,0:T(8,128)(2,1)S(1)}, bf16[96,512]{1,0:T(8,128)(2,1)S(1)}, u32[]{:S(2)}, u32[]{:S(2)}) collective-permute-start(bf16[96,512]{1,0:T(8,128)(2,1)S(1)} %get-tuple-element.50), channel_id=1, source_target_pairs={{0,8},{4,12},{8,0},{12,4},{16,24},{20,28},{24,16},{28,20},{1,9},{5... | collective-permute-start | bytes 294920 | tf_op jit(solution)/shard_map/ppermute | solution.py:40
  33.6 2.9 %collective-permute-done.12 = bf16[96,512]{1,0:T(8,128)(2,1)S(1)} collective-permute-done((bf16[96,512]{1,0:T(8,128)(2,1)S(1)}, bf16[96,512]{1,0:T(8,128)(2,1)S(1)}, u32[]{:S(2)}, u32[]{:S(2)}) %collective-permute-start.12) | collective-permute-done | bytes 98336 | tf_op jit(solution)/shard_map/ppermute | solution.py:40
  39.5 9.1 %collective-permute-done.8.refs_2_.refs_6_ = bf16[384,512]{1,0:T(8,128)(2,1)S(1)} collective-permute-done((bf16[384,512]{1,0:T(8,128)(2,1)S(1)}, bf16[384,512]{1,0:T(8,128)(2,1)S(1)}, u32[]{:S(2)}, u32[]{:S(2)}) %collective-permute-start.8) | collective-permute-done | bytes 393248 | tf_op jit(solution)/shard_map/ppermute | solution.py:40
  51.7 1.8 %mixer.1 = (f32[256,128]{1,0:T(8,128)S(1)}, bf16[256,128]{1,0:T(8,128)(2,1)}, bf16[8,128,256]{2,1,0:T(8,128)(2,1)S(1)}) custom-call(s32[2]{0:T(128)S(1)} %pad_add_fusion.ids, bf16[256,512]{1,0:T(8,128)(2,1)S(1)} %copy-done.6, bf16[256,512]{1,0:T(8,128)(2,1)S(1)} %collective-permute-done.27.refs_1_, bf16[256,512]{1,0:T(8,128)(2,1)S(1)} %collective-permute-done.28.refs_2_, ...), custom_call_target="tpu_custom_call" | custom-call | flops 268435456 | bytes 2097152 | tf_op jit(solution)/shard_map/mixer/pallas_call | solution.py:386
  53.5 1.8 %collective-permute-done.14.refs_2_.refs_10_ = bf16[384,512]{1,0:T(8,128)(2,1)S(1)} collective-permute-done((bf16[384,512]{1,0:T(8,128)(2,1)S(1)}, bf16[384,512]{1,0:T(8,128)(2,1)S(1)}, u32[]{:S(2)}, u32[]{:S(2)}) %collective-permute-start.14) | collective-permute-done | bytes 393248 | tf_op jit(solution)/shard_map/ppermute | solution.py:40
  60.0 5.5 %gate_up.1 = (bf16[768,512]{1,0:T(8,128)(2,1)S(1)}, f32[768,512]{1,0:T(8,128)S(1)}, f32[768,512]{1,0:T(8,128)S(1)}) custom-call(s32[2]{0:T(128)S(1)} %pad_add_fusion.ids, bf16[768,512]{1,0:T(8,128)(2,1)S(1)} %bitcast.33, bf16[768,512]{1,0:T(8,128)(2,1)} %collective-permute-done.refs_1_, bf16[768,512]{1,0:T(8,128)(2,1)} %collective-permute-done.1.refs_2_, ...), custom_call_target="tpu_custom_call" | custom-call | flops 3221225472 | bytes 8388608 | tf_op jit(solution)/shard_map/gate_up/pallas_call | solution.py:172
  65.5 2.5 %act.2 = (bf16[384,512]{1,0:T(8,128)(2,1)S(1)}, bf16[384,512]{1,0:T(8,128)(2,1)S(1)}, bf16[2,384,512]{2,1,0:T(8,128)(2,1)S(1)}) custom-call(s32[2]{0:T(128)S(1)} %pad_add_fusion.ids, bf16[384,512]{1,0:T(8,128)(2,1)S(1)} %constant_dynamic-update-slice_fusion.refs_0_.refs_4_, bf16[384,512]{1,0:T(8,128)(2,1)S(1)} %collective-permute-done.7.refs_1_.refs_5_, ...), custom_call_target="tpu_custom_call" | custom-call | flops 1610612736 | bytes 12582912 | tf_op jit(solution)/shard_map/act/pallas_call | solution.py:206
  68.1 3.0 %collective-permute-start.30 = (bf16[4,128,256]{2,1,0:T(8,128)(2,1)S(1)}, bf16[4,128,256]{2,1,0:T(8,128)(2,1)S(1)}, u32[]{:S(2)}, u32[]{:S(2)}) collective-permute-start(bf16[4,128,256]{2,1,0:T(8,128)(2,1)S(1)} %slice.37), channel_id=1, source_target_pairs={{0,16},{4,20},{8,24},{12,28},{16,0},{20,4},{24,8},{28,12},{1,17},{... | collective-permute-start | bytes 786440 | tf_op jit(solution)/shard_map/ppermute | solution.py:40
  71.2 2.5 %act.3 = (bf16[384,512]{1,0:T(8,128)(2,1)S(1)}, bf16[384,512]{1,0:T(8,128)(2,1)S(1)}, bf16[2,384,512]{2,1,0:T(8,128)(2,1)S(1)}) custom-call(s32[2]{0:T(128)S(1)} %pad_add_fusion.ids, bf16[384,512]{1,0:T(8,128)(2,1)S(1)} %constant_dynamic-update-slice_fusion.4.refs_0_.refs_8_, bf16[384,512]{1,0:T(8,128)(2,1)S(1)} %collective-permute-done.13.refs_1_.refs_9_, ...), custom_call_target="tpu_custom_call" | custom-call | flops 1610612736 | bytes 12582912 | tf_op jit(solution)/shard_map/act/pallas_call | solution.py:206
  73.9 9.8 %collective-permute-done.30 = bf16[4,128,256]{2,1,0:T(8,128)(2,1)S(1)} collective-permute-done((bf16[4,128,256]{2,1,0:T(8,128)(2,1)S(1)}, bf16[4,128,256]{2,1,0:T(8,128)(2,1)S(1)}, u32[]{:S(2)}, u32[]{:S(2)}) %collective-permute-start.30) | collective-permute-done | bytes 262176 | tf_op jit(solution)/shard_map/ppermute | solution.py:40
  89.2 2.1 %collective-permute-start.32 = (bf16[1,128,256]{2,1,0:T(8,128)(2,1)S(1)}, bf16[1,128,256]{2,1,0:T(8,128)(2,1)S(1)}, u32[]{:S(2)}, u32[]{:S(2)}) collective-permute-start(bf16[1,128,256]{2,1,0:T(8,128)(2,1)S(1)} %slice.51), channel_id=1, source_target_pairs={{0,4},{4,0},{8,12},{12,8},{16,20},{20,16},{24,28},{28,24},{1,5},{5... | collective-permute-start | bytes 196616 | tf_op jit(solution)/shard_map/ppermute | solution.py:40
  95.2 3.8 %collective-permute-done.22.refs_0_ = bf16[384,512]{1,0:T(8,128)(2,1)S(1)} collective-permute-done((bf16[384,512]{1,0:T(8,128)(2,1)S(1)}, bf16[384,512]{1,0:T(8,128)(2,1)S(1)}, u32[]{:S(2)}, u32[]{:S(2)}) %collective-permute-start.22) | collective-permute-done | bytes 393248 | tf_op jit(solution)/shard_map/ppermute | solution.py:40
  99.0 3.4 %collective-permute-start.23 = (bf16[96,512]{1,0:T(8,128)(2,1)S(1)}, bf16[96,512]{1,0:T(8,128)(2,1)S(1)}, u32[]{:S(2)}, u32[]{:S(2)}) collective-permute-start(bf16[96,512]{1,0:T(8,128)(2,1)S(1)} %get-tuple-element.73), channel_id=1, source_target_pairs={{0,16},{4,20},{8,24},{12,28},{16,0},{20,4},{24,8},{28,12},{1,17},{... | collective-permute-start | bytes 294920 | tf_op jit(solution)/shard_map/ppermute | solution.py:40
  104.2 2.3 %collective-permute-start.25 = (bf16[96,512]{1,0:T(8,128)(2,1)S(1)}, bf16[96,512]{1,0:T(8,128)(2,1)S(1)}, u32[]{:S(2)}, u32[]{:S(2)}) collective-permute-start(bf16[96,512]{1,0:T(8,128)(2,1)S(1)} %get-tuple-element.75), channel_id=1, source_target_pairs={{0,24},{4,28},{8,16},{12,20},{16,8},{20,12},{24,0},{28,4},{1,25},{... | collective-permute-start | bytes 294920 | tf_op jit(solution)/shard_map/ppermute | solution.py:40
  109.7 3.0 %collective-permute-done.23.refs_4_ = bf16[96,512]{1,0:T(8,128)(2,1)S(1)} collective-permute-done((bf16[96,512]{1,0:T(8,128)(2,1)S(1)}, bf16[96,512]{1,0:T(8,128)(2,1)S(1)}, u32[]{:S(2)}, u32[]{:S(2)}) %collective-permute-start.23) | collective-permute-done | bytes 98336 | tf_op jit(solution)/shard_map/ppermute | solution.py:40
  112.6 3.4 %collective-permute-done.24.refs_5_ = bf16[96,512]{1,0:T(8,128)(2,1)S(1)} collective-permute-done((bf16[96,512]{1,0:T(8,128)(2,1)S(1)}, bf16[96,512]{1,0:T(8,128)(2,1)S(1)}, u32[]{:S(2)}, u32[]{:S(2)}) %collective-permute-start.24) | collective-permute-done | bytes 98336 | tf_op jit(solution)/shard_map/ppermute | solution.py:40
  116.0 8.1 %weight_grads.1 = (bf16[2048,512]{1,0:T(8,128)(2,1)}, bf16[2048,512]{1,0:T(8,128)(2,1)}, bf16[512,2048]{1,0:T(8,128)(2,1)}) custom-call(s32[2]{0:T(128)S(1)} %pad_add_fusion.ids, bf16[768,512]{1,0:T(8,128)(2,1)S(1)} %bitcast.34, bf16[768,512]{1,0:T(8,128)(2,1)} %collective-permute-done.refs_1_, bf16[768,512]{1,0:T(8,128)(2,1)} %collective-permute-done.1.refs_2_, ...), custom_call_target="tpu_custom_call" | custom-call | flops 4831838208 | bytes 18874368 | tf_op jit(solution)/shard_map/weight_grads/pallas_call | solution.py:341
  (107 shorter events, 35.1 us)
Async XLA Ops:
  0.7 31.2 %collective-permute-start.1 = (bf16[768,512]{1,0:T(8,128)(2,1)}, bf16[768,512]{1,0:T(8,128)(2,1)}, u32[]{:S(2)}, u32[]{:S(2)}) collective-permute-start(bf16[768,512]{1,0:T(8,128)(2,1)} %bitcast.31), channel_id=1, source_target_pairs={{0,2},{1,3},{2,0},{3,1},{4,6},{5,7},{6,4},{7,5},{8,10},{9,11},{10,... | collective-permute-start | bytes 2359304 | tf_op jit(solution)/shard_map/ppermute | solution.py:40
  3.7 51.6 %collective-permute-start = (bf16[768,512]{1,0:T(8,128)(2,1)}, bf16[768,512]{1,0:T(8,128)(2,1)}, u32[]{:S(2)}, u32[]{:S(2)}) collective-permute-start(bf16[768,512]{1,0:T(8,128)(2,1)} %bitcast.32), channel_id=1, source_target_pairs={{0,1},{1,0},{2,3},{3,2},{4,5},{5,4},{6,7},{7,6},{8,9},{9,8},{10,11... | collective-permute-start | bytes 2359304 | tf_op jit(solution)/shard_map/ppermute | solution.py:40
  3.7 34.4 %collective-permute-start.28 = (bf16[256,512]{1,0:T(8,128)(2,1)}, bf16[256,512]{1,0:T(8,128)(2,1)S(1)}, u32[]{:S(2)}, u32[]{:S(2)}) collective-permute-start(bf16[256,512]{1,0:T(8,128)(2,1)} %refs_0_.1), channel_id=1, source_target_pairs={{0,2},{1,3},{2,0},{3,1},{4,6},{5,7},{6,4},{7,5},{8,10},{9,11},{10,... | collective-permute-start | bytes 786440 | tf_op jit(solution)/shard_map/ppermute | solution.py:40
  10.5 11.0 %collective-permute-start.4 = (bf16[96,512]{1,0:T(8,128)(2,1)S(1)}, bf16[96,512]{1,0:T(8,128)(2,1)S(1)}, u32[]{:S(2)}, u32[]{:S(2)}) collective-permute-start(bf16[96,512]{1,0:T(8,128)(2,1)S(1)} %get-tuple-element.45), channel_id=1, source_target_pairs={{0,20},{4,16},{8,28},{12,24},{16,4},{20,0},{24,12},{28,8},{1,21},{... | collective-permute-start | bytes 294920 | tf_op jit(solution)/shard_map/ppermute | solution.py:40
  31.9 24.0 %collective-permute-start.2 = (bf16[768,512]{1,0:T(8,128)(2,1)}, bf16[768,512]{1,0:T(8,128)(2,1)S(1)}, u32[]{:S(2)}, u32[]{:S(2)}) collective-permute-start(bf16[768,512]{1,0:T(8,128)(2,1)} %collective-permute-done.1.refs_2_), channel_id=1, source_target_pairs={{0,1},{1,0},{2,3},{3,2},{4,5},{5,4},{6,7},{7,6},{8,9},{9,8},{10,11... | collective-permute-start | bytes 2359304 | tf_op jit(solution)/shard_map/ppermute | solution.py:40
  36.6 12.0 %collective-permute-start.8 = (bf16[384,512]{1,0:T(8,128)(2,1)S(1)}, bf16[384,512]{1,0:T(8,128)(2,1)S(1)}, u32[]{:S(2)}, u32[]{:S(2)}) collective-permute-start(bf16[384,512]{1,0:T(8,128)(2,1)S(1)} %constant_dynamic-update-slice_fusion.refs_0_.refs_4_), channel_id=1, source_target_pairs={{0,2},{1,3},{2,0},{3,1},{4,6},{5,7},{6,4},{7,5},{8,10},{9,11},{10,... | collective-permute-start | bytes 1179656 | tf_op jit(solution)/shard_map/ppermute | solution.py:40
  38.2 17.1 %collective-permute-start.14 = (bf16[384,512]{1,0:T(8,128)(2,1)S(1)}, bf16[384,512]{1,0:T(8,128)(2,1)S(1)}, u32[]{:S(2)}, u32[]{:S(2)}) collective-permute-start(bf16[384,512]{1,0:T(8,128)(2,1)S(1)} %constant_dynamic-update-slice_fusion.4.refs_0_.refs_8_), channel_id=1, source_target_pairs={{0,2},{1,3},{2,0},{3,1},{4,6},{5,7},{6,4},{7,5},{8,10},{9,11},{10,... | collective-permute-start | bytes 1179656 | tf_op jit(solution)/shard_map/ppermute | solution.py:40
  48.5 17.0 %collective-permute-start.7 = (bf16[384,512]{1,0:T(8,128)(2,1)S(1)}, bf16[384,512]{1,0:T(8,128)(2,1)S(1)}, u32[]{:S(2)}, u32[]{:S(2)}) collective-permute-start(bf16[384,512]{1,0:T(8,128)(2,1)S(1)} %constant_dynamic-update-slice_fusion.refs_0_.refs_4_), channel_id=1, source_target_pairs={{0,1},{1,0},{2,3},{3,2},{4,5},{5,4},{6,7},{7,6},{8,9},{9,8},{10,11... | collective-permute-start | bytes 1179656 | tf_op jit(solution)/shard_map/ppermute | solution.py:40
  48.6 17.0 %collective-permute-start.9 = (bf16[384,512]{1,0:T(8,128)(2,1)S(1)}, bf16[384,512]{1,0:T(8,128)(2,1)S(1)}, u32[]{:S(2)}, u32[]{:S(2)}) collective-permute-start(bf16[384,512]{1,0:T(8,128)(2,1)S(1)} %collective-permute-done.8.refs_2_.refs_6_), channel_id=1, source_target_pairs={{0,1},{1,0},{2,3},{3,2},{4,5},{5,4},{6,7},{7,6},{8,9},{9,8},{10,11... | collective-permute-start | bytes 1179656 | tf_op jit(solution)/shard_map/ppermute | solution.py:40
  55.3 15.9 %collective-permute-start.13 = (bf16[384,512]{1,0:T(8,128)(2,1)S(1)}, bf16[384,512]{1,0:T(8,128)(2,1)S(1)}, u32[]{:S(2)}, u32[]{:S(2)}) collective-permute-start(bf16[384,512]{1,0:T(8,128)(2,1)S(1)} %constant_dynamic-update-slice_fusion.4.refs_0_.refs_8_), channel_id=1, source_target_pairs={{0,1},{1,0},{2,3},{3,2},{4,5},{5,4},{6,7},{7,6},{8,9},{9,8},{10,11... | collective-permute-start | bytes 1179656 | tf_op jit(solution)/shard_map/ppermute | solution.py:40
  55.3 15.9 %collective-permute-start.15 = (bf16[384,512]{1,0:T(8,128)(2,1)S(1)}, bf16[384,512]{1,0:T(8,128)(2,1)S(1)}, u32[]{:S(2)}, u32[]{:S(2)}) collective-permute-start(bf16[384,512]{1,0:T(8,128)(2,1)S(1)} %collective-permute-done.14.refs_2_.refs_10_), channel_id=1, source_target_pairs={{0,1},{1,0},{2,3},{3,2},{4,5},{5,4},{6,7},{7,6},{8,9},{9,8},{10,11... | collective-permute-start | bytes 1179656 | tf_op jit(solution)/shard_map/ppermute | solution.py:40
  55.8 15.3 %collective-permute-start.33 = (f32[2,128]{1,0:T(2,128)S(1)}, f32[2,128]{1,0:T(2,128)S(1)}, u32[]{:S(2)}, u32[]{:S(2)}) collective-permute-start(f32[2,128]{1,0:T(2,128)S(1)} %slice.43), channel_id=1, source_target_pairs={{4,0},{8,4},{12,8},{16,12},{20,16},{24,20},{28,24},{5,1},{9,5},{13... | collective-permute-start | bytes 3080 | tf_op jit(solution)/shard_map/ppermute | solution.py:46
  68.0 17.3 %collective-permute-start.21 = (bf16[2,384,512]{2,1,0:T(8,128)(2,1)S(1)}, bf16[2,384,512]{2,1,0:T(8,128)(2,1)S(1)}, u32[]{:S(2)}, u32[]{:S(2)}) collective-permute-start(bf16[2,384,512]{2,1,0:T(8,128)(2,1)S(1)} %get-tuple-element.70), channel_id=1, source_target_pairs={{0,1},{1,0},{2,3},{3,2},{4,5},{5,4},{6,7},{7,6},{8,9},{9,8},{10,11... | collective-permute-start | bytes 2359304 | tf_op jit(solution)/shard_map/ppermute | solution.py:40
  68.1 15.6 %collective-permute-start.30 = (bf16[4,128,256]{2,1,0:T(8,128)(2,1)S(1)}, bf16[4,128,256]{2,1,0:T(8,128)(2,1)S(1)}, u32[]{:S(2)}, u32[]{:S(2)}) collective-permute-start(bf16[4,128,256]{2,1,0:T(8,128)(2,1)S(1)} %slice.37), channel_id=1, source_target_pairs={{0,16},{4,20},{8,24},{12,28},{16,0},{20,4},{24,8},{28,12},{1,17},{... | collective-permute-start | bytes 786440 | tf_op jit(solution)/shard_map/ppermute | solution.py:40
  73.6 17.7 %collective-permute-start.16 = (bf16[2,384,512]{2,1,0:T(8,128)(2,1)S(1)}, bf16[2,384,512]{2,1,0:T(8,128)(2,1)S(1)}, u32[]{:S(2)}, u32[]{:S(2)}) collective-permute-start(bf16[2,384,512]{2,1,0:T(8,128)(2,1)S(1)} %get-tuple-element.63), channel_id=1, source_target_pairs={{0,1},{1,0},{2,3},{3,2},{4,5},{5,4},{6,7},{7,6},{8,9},{9,8},{10,11... | collective-permute-start | bytes 2359304 | tf_op jit(solution)/shard_map/ppermute | solution.py:40
  86.9 12.1 %collective-permute-start.22 = (bf16[384,512]{1,0:T(8,128)(2,1)S(1)}, bf16[384,512]{1,0:T(8,128)(2,1)S(1)}, u32[]{:S(2)}, u32[]{:S(2)}) collective-permute-start(bf16[384,512]{1,0:T(8,128)(2,1)S(1)} %get-tuple-element.72), channel_id=1, source_target_pairs={{0,2},{1,3},{2,0},{3,1},{4,6},{5,7},{6,4},{7,5},{8,10},{9,11},{10,... | collective-permute-start | bytes 1179656 | tf_op jit(solution)/shard_map/ppermute | solution.py:40
  89.2 14.3 %collective-permute-start.32 = (bf16[1,128,256]{2,1,0:T(8,128)(2,1)S(1)}, bf16[1,128,256]{2,1,0:T(8,128)(2,1)S(1)}, u32[]{:S(2)}, u32[]{:S(2)}) collective-permute-start(bf16[1,128,256]{2,1,0:T(8,128)(2,1)S(1)} %slice.51), channel_id=1, source_target_pairs={{0,4},{4,0},{8,12},{12,8},{16,20},{20,16},{24,28},{28,24},{1,5},{5... | collective-permute-start | bytes 196616 | tf_op jit(solution)/shard_map/ppermute | solution.py:40
  92.9 15.0 %collective-permute-start.17 = (bf16[384,512]{1,0:T(8,128)(2,1)S(1)}, bf16[384,512]{1,0:T(8,128)(2,1)S(1)}, u32[]{:S(2)}, u32[]{:S(2)}) collective-permute-start(bf16[384,512]{1,0:T(8,128)(2,1)S(1)} %get-tuple-element.65), channel_id=1, source_target_pairs={{0,2},{1,3},{2,0},{3,1},{4,6},{5,7},{6,4},{7,5},{8,10},{9,11},{10,... | collective-permute-start | bytes 1179656 | tf_op jit(solution)/shard_map/ppermute | solution.py:40
  99.0 13.6 %collective-permute-start.23 = (bf16[96,512]{1,0:T(8,128)(2,1)S(1)}, bf16[96,512]{1,0:T(8,128)(2,1)S(1)}, u32[]{:S(2)}, u32[]{:S(2)}) collective-permute-start(bf16[96,512]{1,0:T(8,128)(2,1)S(1)} %get-tuple-element.73), channel_id=1, source_target_pairs={{0,16},{4,20},{8,24},{12,28},{16,0},{20,4},{24,8},{28,12},{1,17},{... | collective-permute-start | bytes 294920 | tf_op jit(solution)/shard_map/ppermute | solution.py:40
  102.4 13.6 %collective-permute-start.24 = (bf16[96,512]{1,0:T(8,128)(2,1)S(1)}, bf16[96,512]{1,0:T(8,128)(2,1)S(1)}, u32[]{:S(2)}, u32[]{:S(2)}) collective-permute-start(bf16[96,512]{1,0:T(8,128)(2,1)S(1)} %get-tuple-element.74), channel_id=1, source_target_pairs={{0,20},{4,16},{8,28},{12,24},{16,4},{20,0},{24,12},{28,8},{1,21},{... | collective-permute-start | bytes 294920 | tf_op jit(solution)/shard_map/ppermute | solution.py:40
  104.2 20.0 %collective-permute-start.25 = (bf16[96,512]{1,0:T(8,128)(2,1)S(1)}, bf16[96,512]{1,0:T(8,128)(2,1)S(1)}, u32[]{:S(2)}, u32[]{:S(2)}) collective-permute-start(bf16[96,512]{1,0:T(8,128)(2,1)S(1)} %get-tuple-element.75), channel_id=1, source_target_pairs={{0,24},{4,28},{8,16},{12,20},{16,8},{20,12},{24,0},{28,4},{1,25},{... | collective-permute-start | bytes 294920 | tf_op jit(solution)/shard_map/ppermute | solution.py:40
  106.5 17.7 %collective-permute-start.26 = (bf16[96,512]{1,0:T(8,128)(2,1)S(1)}, bf16[96,512]{1,0:T(8,128)(2,1)S(1)}, u32[]{:S(2)}, u32[]{:S(2)}) collective-permute-start(bf16[96,512]{1,0:T(8,128)(2,1)S(1)} %get-tuple-element.76), channel_id=1, source_target_pairs={{0,28},{4,24},{8,20},{12,16},{16,12},{20,8},{24,4},{28,0},{1,29},{... | collective-permute-start | bytes 294920 | tf_op jit(solution)/shard_map/ppermute | solution.py:40
  108.1 16.2 %collective-permute-start.18 = (bf16[96,512]{1,0:T(8,128)(2,1)S(1)}, bf16[96,512]{1,0:T(8,128)(2,1)S(1)}, u32[]{:S(2)}, u32[]{:S(2)}) collective-permute-start(bf16[96,512]{1,0:T(8,128)(2,1)S(1)} %get-tuple-element.67), channel_id=1, source_target_pairs={{0,4},{4,0},{8,12},{12,8},{16,20},{20,16},{24,28},{28,24},{1,5},{5... | collective-permute-start | bytes 294920 | tf_op jit(solution)/shard_map/ppermute | solution.py:40
  112.6 11.6 %collective-permute-start.19 = (bf16[96,512]{1,0:T(8,128)(2,1)S(1)}, bf16[96,512]{1,0:T(8,128)(2,1)S(1)}, u32[]{:S(2)}, u32[]{:S(2)}) collective-permute-start(bf16[96,512]{1,0:T(8,128)(2,1)S(1)} %get-tuple-element.68), channel_id=1, source_target_pairs={{0,8},{4,12},{8,0},{12,4},{16,24},{20,28},{24,16},{28,20},{1,9},{5... | collective-permute-start | bytes 294920 | tf_op jit(solution)/shard_map/ppermute | solution.py:40
  (25 other events, 233.3 us)
